TPU v7x, 32 devices: a whole 2x2x4 slice. The times are simulated.
32 devices in a mesh: sp: 4 (over z), dp: 8 (over y, x, core).
Axes of the slice: x: 2, y: 2, z: 4, core: 2. Of those that a mesh axis runs over, the one named last changes fastest.
Arguments:
- queries: bfloat16 [8, 768, 6144], P('dp', None, 'sp'), may hold values from -64 to 64
- out_grad: bfloat16 [8, 768, 4096], P('dp', None, 'sp'), may hold values from -6 to 6
- latent: bfloat16 [8, 768, 512], P('dp'), may hold values from -6 to 6
- rope_key: bfloat16 [8, 768, 64], P('dp'), may hold values from -6 to 6
- kv_gain: float32 [512], replicated, may hold values from 0.1 to 1.9
- key_up: bfloat16 [512, 4096], P('dp', 'sp'), may hold values from -0.25 to 0.25
- value_up: bfloat16 [512, 4096], P('dp', 'sp'), may hold values from -0.25 to 0.25
Outputs:
- query_grad: bfloat16 [8, 768, 6144], P('dp', None, 'sp')
- latent_grad: bfloat16 [8, 768, 512], P('dp')
- rope_key_grad: bfloat16 [8, 768, 64], P('dp')
- key_up_grad: float32 [512, 4096], P('dp', 'sp')
- value_up_grad: float32 [512, 4096], P('dp', 'sp')
All inputs are finite; a program needn't handle non-finite values.
Results may differ from a plain program's by a relative error of at most 0.019.
The roundings to bfloat16 on the way count: a program that leaves them out, or rounds other values in their place, can miss the bound.
Values may be sent and summed in bfloat16 or wider, within the bound.
A program may use at most 64 MiB of HBM per device.

v0:
```python
import functools

import jax
import jax.numpy as jnp
import numpy as np
from jax import lax
from jax.experimental import pallas as pl
from jax.experimental.pallas import tpu as pltpu
from jax.sharding import PartitionSpec as P

NOPE_DIM = 128
ROPE_DIM = 64
VALUE_DIM = 128
QK = NOPE_DIM + ROPE_DIM
LOG2E = 1.4426950408889634

norm_eps = 1e-06
rope_theta = 10000.0

NT = (((1,), (1,)), ((), ()))


def rope_tables(length):
    half = ROPE_DIM // 2
    frequency = np.float32(rope_theta) ** (-(np.arange(half, dtype=np.float32) * np.float32(2.0 / ROPE_DIM)))
    angles = np.arange(length, dtype=np.float32)[:, None] * frequency.astype(np.float32)[None, :]
    return np.cos(angles).astype(np.float32), np.sin(angles).astype(np.float32)


def dot(a, b):
    return jnp.dot(a, b, preferred_element_type=jnp.float32)


def dot_nt(a, b):
    return lax.dot_general(a, b, NT, preferred_element_type=jnp.float32)


def swap_halves(x):
    lane = lax.broadcasted_iota(jnp.int32, x.shape, 1)
    return jnp.where(lane % ROPE_DIM < ROPE_DIM // 2, pltpu.roll(x, 96, 1), pltpu.roll(x, 32, 1))


def attention_kernel(
    block, grad_scale,
    latent_ref, rope_ref, gain_ref, cos_ref, sin_ref, cos_t_ref, sin_t_ref,
    q_ref, do_ref, wk_ref, wv_ref,
    dq_ref, dw_ref, part_ref,
    comp, comp_t, krot, krot_t, ku, kt, vals, qu, pt, dst, dkv, acc, rot_acc,
):
    step = pl.program_id(0)
    length = q_ref.shape[0]
    tiles = length // block
    scale = QK ** (-0.5)

    @pl.when(step == 0)
    def _():
        raw = latent_ref[...].astype(jnp.float32)
        inverse = lax.rsqrt(jnp.mean(raw * raw, axis=-1, keepdims=True) + norm_eps)
        normed = raw * inverse * gain_ref[...]
        comp[...] = normed.astype(jnp.bfloat16)
        comp_t[...] = normed.T.astype(jnp.bfloat16)
        rope = rope_ref[...].astype(jnp.float32)
        wide = jnp.concatenate([rope, rope], axis=1)
        turned = wide * cos_ref[...] + swap_halves(wide) * sin_ref[...]
        krot[...] = turned.astype(jnp.bfloat16)
        krot_t[...] = turned.T.astype(jnp.bfloat16)
        acc[...] = jnp.zeros_like(acc)
        rot_acc[...] = jnp.zeros_like(rot_acc)

    keys = dot(comp[...], wk_ref[...])
    keys_t = keys.T.astype(jnp.bfloat16)
    keys = keys.astype(jnp.bfloat16)
    vals[...] = dot(comp[...], wv_ref[...]).astype(jnp.bfloat16)
    for h in range(2):
        ku[h, :, :NOPE_DIM] = keys[:, h * NOPE_DIM:(h + 1) * NOPE_DIM]
        ku[h, :, NOPE_DIM:] = krot[:, :ROPE_DIM]
        kt[h, :NOPE_DIM, :] = keys_t[h * NOPE_DIM:(h + 1) * NOPE_DIM, :]
        kt[h, NOPE_DIM:, :] = krot_t[:ROPE_DIM, :]

    mid = q_ref[:, 128:256].astype(jnp.float32)
    last = q_ref[:, 256:384].astype(jnp.float32)
    low = lax.broadcasted_iota(jnp.int32, mid.shape, 1) < 64
    plain = jnp.where(low, pltpu.roll(mid, 64, 1), pltpu.roll(last, 64, 1))
    rope = jnp.where(low, mid, last)
    turned = rope * cos_ref[...] + swap_halves(rope) * sin_ref[...]
    qu[0, :, :NOPE_DIM] = q_ref[:, :128]
    qu[0, :, NOPE_DIM:] = turned[:, :ROPE_DIM].astype(jnp.bfloat16)
    qu[1, :, :NOPE_DIM] = plain.astype(jnp.bfloat16)
    qu[1, :, NOPE_DIM:] = pltpu.roll(turned, 64, 1)[:, :ROPE_DIM].astype(jnp.bfloat16)

    for i in range(tiles):
        rows = slice(i * block, (i + 1) * block)
        n = (i + 1) * block
        parts = []
        for h in range(2):
            cols = slice(h * VALUE_DIM, (h + 1) * VALUE_DIM)
            scores = dot_nt(ku[h, :n, :], qu[h, rows, :])
            key_at = lax.broadcasted_iota(jnp.int32, (block, block), 0)
            query_at = lax.broadcasted_iota(jnp.int32, (block, block), 1)
            diag = jnp.where(key_at <= query_at, scores[n - block:], -jnp.inf)
            scores = diag if i == 0 else jnp.concatenate([scores[:n - block], diag], axis=0)
            top = jnp.max(scores, axis=0, keepdims=True)
            e = jnp.exp2((scores - top) * (scale * LOG2E))
            r = 1.0 / jnp.sum(e, axis=0, keepdims=True)
            prob_grad = dot_nt(vals[:n, cols], do_ref[rows, cols])
            center = jnp.sum(e * prob_grad, axis=0, keepdims=True) * r
            pt[h, :n, rows] = (e * r).astype(jnp.bfloat16)
            ds = (e * (r * scale) * (prob_grad - center)).astype(jnp.bfloat16)
            dst[h, :n, rows] = ds
            g = dot(kt[h, :, :n], ds)
            a = g[NOPE_DIM:NOPE_DIM + 32]
            b = g[NOPE_DIM + 32:]
            c, s = cos_t_ref[:, rows], sin_t_ref[:, rows]
            parts += [g[:NOPE_DIM], a * c + b * s, b * c - a * s]
        dq_ref[rows, :] = jnp.concatenate(parts, axis=0).T.astype(jnp.bfloat16)

    for h in range(2):
        for j in range(tiles):
            rows = slice(j * block, (j + 1) * block)
            cols = slice(h * VALUE_DIM, (h + 1) * VALUE_DIM)
            dv = dot(pt[h, rows, j * block:], do_ref[j * block:, cols])
            dk = dot(dst[h, rows, j * block:], qu[h, j * block:, :])
            dkv[rows, h * NOPE_DIM:(h + 1) * NOPE_DIM] = dk[:, :NOPE_DIM].astype(jnp.bfloat16)
            dkv[rows, (2 + h) * 128:(3 + h) * 128] = dv.astype(jnp.bfloat16)
            rot_acc[rows, :] += dk[:, NOPE_DIM:]

    dw = dot(comp_t[...], dkv[...]) * grad_scale
    dw_ref[:, 0] = dw[:, :256].reshape(dw_ref.shape[0], dw_ref.shape[2], 256).astype(dw_ref.dtype)
    dw_ref[:, 1] = dw[:, 256:].reshape(dw_ref.shape[0], dw_ref.shape[2], 256).astype(dw_ref.dtype)
    acc[...] += dot_nt(dkv[:, :256], wk_ref[...]) + dot_nt(dkv[:, 256:], wv_ref[...])

    @pl.when(step == pl.num_programs(0) - 1)
    def _():
        width = acc.shape[1]
        rot = rot_acc[...].astype(jnp.bfloat16)
        part_ref[:, :width] = acc[...].astype(jnp.bfloat16)
        part_ref[:, width:] = jnp.concatenate([rot, rot], axis=1)


def attention(queries, out_grad, latent, rope_key, kv_gain, key_whole, value_whole, grad_scale, n_dp):
    length = queries.shape[0]
    width = latent.shape[1]
    pairs = key_whole.shape[1] // 256
    block = 256
    cosine, sine = rope_tables(length)
    cos_wide = np.tile(cosine, (1, 4))
    sin_wide = np.concatenate([-sine, sine, -sine, sine], axis=1)
    bf, f32 = jnp.bfloat16, jnp.float32
    whole = lambda shape: pl.BlockSpec(shape, lambda p: (0,) * len(shape))
    column = lambda rows, cols: pl.BlockSpec((rows, cols), lambda p: (0, p))
    return pl.pallas_call(
        functools.partial(attention_kernel, block, grad_scale),
        grid=(pairs,),
        in_specs=[
            whole((length, width)), whole((length, ROPE_DIM)), whole((1, width)),
            whole((length, 128)), whole((length, 128)),
            whole((32, length)), whole((32, length)),
            column(length, 2 * QK), column(length, 256), column(width, 256), column(width, 256),
        ],
        out_specs=[
            column(length, 2 * QK),
            pl.BlockSpec((n_dp, 2, width // n_dp, 256), lambda p: (0, 0, 0, p)),
            whole((length, width + 128)),
        ],
        out_shape=[
            jax.ShapeDtypeStruct(queries.shape, bf),
            jax.ShapeDtypeStruct((n_dp, 2, width // n_dp, key_whole.shape[1]), bf),
            jax.ShapeDtypeStruct((length, width + 128), bf),
        ],
        scratch_shapes=[
            pltpu.VMEM((length, width), bf), pltpu.VMEM((width, length), bf),
            pltpu.VMEM((length, 128), bf), pltpu.VMEM((128, length), bf),
            pltpu.VMEM((2, length, QK), bf), pltpu.VMEM((2, QK, length), bf),
            pltpu.VMEM((length, 256), bf), pltpu.VMEM((2, length, QK), bf),
            pltpu.VMEM((2, length, length), bf), pltpu.VMEM((2, length, length), bf),
            pltpu.VMEM((length, 512), bf),
            pltpu.VMEM((length, width), f32), pltpu.VMEM((length, ROPE_DIM), f32),
        ],
        compiler_params=pltpu.CompilerParams(
            dimension_semantics=("arbitrary",), vmem_limit_bytes=48 * 1024 * 1024
        ),
        cost_estimate=pl.CostEstimate(flops=10_000_000_000, bytes_accessed=12_000_000, transcendentals=4_000_000),
        name="attention_backward",
    )(
        latent, rope_key, kv_gain.reshape(1, -1), cos_wide, sin_wide,
        np.ascontiguousarray(cosine.T), np.ascontiguousarray(sine.T),
        queries, out_grad, key_whole, value_whole,
    )


def exchange_kernel(
    n_sp, n_dp,
    dw_ref, part_ref, latent_ref, gain_ref, cos_ref, sin_ref,
    grad_ref, low_ref,
    got_part, got_dw, send_a, recv_a, send_b, recv_b, send_c, recv_c,
):
    sp, dp = lax.axis_index("sp"), lax.axis_index("dp")
    rows = latent_ref.shape[0] // n_sp
    width = latent_ref.shape[1]
    mine = pl.ds(pl.multiple_of(sp * rows, rows), rows)
    mesh_id = pl.DeviceIdType.MESH
    barrier = pltpu.get_barrier_semaphore()

    def each(count, act):
        def body(k, carry):
            act(k)
            return carry
        lax.fori_loop(1, count, body, 0)

    def greet(axis, here, count):
        each(count, lambda k: pl.semaphore_signal(
            barrier, inc=1, device_id={axis: lax.rem(here + k, count)}, device_id_type=mesh_id))

    greet("sp", sp, n_sp)
    greet("dp", dp, n_dp)
    pl.semaphore_wait(barrier, n_sp + n_dp - 2)

    def part_copy(k):
        peer = lax.rem(sp + k, n_sp)
        return pltpu.make_async_remote_copy(
            src_ref=part_ref.at[pl.ds(pl.multiple_of(peer * rows, rows), rows)],
            dst_ref=got_part.at[k], send_sem=send_a.at[k], recv_sem=recv_a.at[k],
            device_id={"sp": peer}, device_id_type=mesh_id)

    def dw_copy(k):
        peer = lax.rem(dp + k, n_dp)
        return pltpu.make_async_remote_copy(
            src_ref=dw_ref.at[peer], dst_ref=got_dw.at[k],
            send_sem=send_b.at[k], recv_sem=recv_b.at[k],
            device_id={"dp": peer}, device_id_type=mesh_id)

    def low_copy(k):
        return pltpu.make_async_remote_copy(
            src_ref=low_ref.at[mine], dst_ref=low_ref.at[mine],
            send_sem=send_c.at[k], recv_sem=recv_c.at[k],
            device_id={"sp": lax.rem(sp + k, n_sp)}, device_id_type=mesh_id)

    each(n_sp, lambda k: part_copy(k).start())
    each(n_dp, lambda k: dw_copy(k).start())

    total = part_ref[mine, :].astype(jnp.float32)
    each(n_sp, lambda k: part_copy(k).wait())
    for k in range(1, n_sp):
        total = total + got_part[k].astype(jnp.float32)
    raw = latent_ref[mine, :].astype(jnp.float32)
    inverse = lax.rsqrt(jnp.mean(raw * raw, axis=-1, keepdims=True) + norm_eps)
    mixed = total[:, :width] * gain_ref[...]
    spread = jnp.mean(raw * mixed, axis=-1, keepdims=True)
    low_ref[mine, :width] = (inverse * mixed - raw * inverse**3 * spread).astype(jnp.bfloat16)
    rot = total[:, width:]
    low_ref[mine, width:] = (
        rot * cos_ref[mine, :] - swap_halves(rot) * sin_ref[mine, :]
    ).astype(jnp.bfloat16)
    each(n_sp, lambda k: low_copy(k).start())

    grad_ref[...] = dw_ref[dp].astype(jnp.float32)
    def add(k):
        dw_copy(k).wait()
        grad_ref[...] += got_dw[k].astype(jnp.float32)
    each(n_dp, add)
    each(n_sp, lambda k: low_copy(k).wait())


def exchange(dw, part, latent, kv_gain, n_sp, n_dp):
    length, width = latent.shape
    cosine, sine = rope_tables(length)
    bf = jnp.bfloat16
    vmem = pl.BlockSpec(memory_space=pltpu.VMEM)
    sems = lambda n: pltpu.SemaphoreType.DMA((n,))
    return pl.pallas_call(
        functools.partial(exchange_kernel, n_sp, n_dp),
        in_specs=[vmem] * 6,
        out_specs=[vmem] * 2,
        out_shape=[
            jax.ShapeDtypeStruct(dw.shape[1:], jnp.float32),
            jax.ShapeDtypeStruct(part.shape, bf),
        ],
        scratch_shapes=[
            pltpu.VMEM((n_sp, length // n_sp, part.shape[1]), bf),
            pltpu.VMEM(dw.shape, bf),
            sems(n_sp), sems(n_sp), sems(n_dp), sems(n_dp), sems(n_sp), sems(n_sp),
        ],
        compiler_params=pltpu.CompilerParams(
            collective_id=0, has_side_effects=True, vmem_limit_bytes=32 * 1024 * 1024
        ),
        name="exchange",
    )(
        dw, part, latent, kv_gain.reshape(1, -1), np.tile(cosine, (1, 4)),
        np.concatenate([-sine, sine, -sine, sine], axis=1),
    )


def gather_kernel(
    n_dp, key_ref, value_ref, key_out, value_out, send_a, recv_a, send_b, recv_b
):
    dp = lax.axis_index("dp")
    chips = n_dp // 2
    chip, core = dp // 2, lax.rem(dp, 2)
    partner = chip * 2 + 1 - core
    mesh_id = pl.DeviceIdType.MESH
    barrier = pltpu.get_barrier_semaphore()
    pairs = ((key_ref, key_out), (value_ref, value_out))

    def each(act):
        def body(k, carry):
            act(k)
            return carry
        lax.fori_loop(1, chips, body, 0)

    def other(k):
        return lax.rem(chip + k, chips) * 2 + core

    def source(k):
        return lax.rem(chip - k + chips, chips) * 2 + core

    each(lambda k: pl.semaphore_signal(
        barrier, inc=1, device_id={"dp": other(k)}, device_id_type=mesh_id))
    pl.semaphore_signal(barrier, inc=1, device_id={"dp": partner}, device_id_type=mesh_id)
    pl.semaphore_wait(barrier, chips)

    def far(t, k):
        return pltpu.make_async_remote_copy(
            src_ref=pairs[t][0], dst_ref=pairs[t][1].at[dp],
            send_sem=send_a.at[t, k], recv_sem=recv_a.at[t, k],
            device_id={"dp": other(k)}, device_id_type=mesh_id)

    def near(t, k, own):
        block = dp if own else source(k)
        return pltpu.make_async_remote_copy(
            src_ref=pairs[t][0] if own else pairs[t][1].at[block],
            dst_ref=pairs[t][1].at[block],
            send_sem=send_b.at[t, k], recv_sem=recv_b.at[t, k],
            device_id={"dp": partner}, device_id_type=mesh_id)

    for t in range(2):
        each(lambda k: far(t, k).start())
    for t in range(2):
        near(t, 0, True).start()
        pairs[t][1][dp] = pairs[t][0][...]

    def forward(k):
        for t in range(2):
            far(t, k).wait_recv()
            near(t, k, False).start()

    def drain(k):
        for t in range(2):
            far(t, k).wait_send()
            near(t, k, False).wait()

    each(forward)
    for t in range(2):
        near(t, 0, True).wait()
    each(drain)


def gather(key_up, value_up, n_dp):
    vmem = pl.BlockSpec(memory_space=pltpu.VMEM)
    shape = jax.ShapeDtypeStruct((n_dp, *key_up.shape), key_up.dtype)
    outs = pl.pallas_call(
        functools.partial(gather_kernel, n_dp),
        in_specs=[vmem] * 2,
        out_specs=[vmem] * 2,
        out_shape=[shape, shape],
        scratch_shapes=[pltpu.SemaphoreType.DMA((2, n_dp // 2))] * 4,
        compiler_params=pltpu.CompilerParams(
            collective_id=1, has_side_effects=True, vmem_limit_bytes=16 * 1024 * 1024
        ),
        name="gather",
    )(key_up, value_up)
    return [out.reshape(n_dp * key_up.shape[0], -1) for out in outs]


def shards(queries, out_grad, latent, rope_key, kv_gain, key_up, value_up):
    length, width = latent.shape[1:]
    n_sp, n_dp = lax.axis_size("sp"), lax.axis_size("dp")
    grad_scale = float(n_dp * length) ** (-0.5)
    key_whole, value_whole = gather(key_up, value_up, n_dp)
    query_grad, dw, part = attention(
        queries[0], out_grad[0], latent[0], rope_key[0], kv_gain, key_whole, value_whole, grad_scale, n_dp
    )
    dw, low = exchange(dw, part, latent[0], kv_gain, n_sp, n_dp)
    return query_grad[None], low[None, :, :width], low[None, :, width:width + ROPE_DIM], dw[0], dw[1]


def solution(mesh):
    return jax.shard_map(
        shards,
        mesh=mesh,
        in_specs=(
            P("dp", None, "sp"),
            P("dp", None, "sp"),
            P("dp", None, None),
            P("dp", None, None),
            P(),
            P("dp", "sp"),
            P("dp", "sp"),
        ),
        out_specs=(
            P("dp", None, "sp"),
            P("dp", None, None),
            P("dp", None, None),
            P("dp", "sp"),
            P("dp", "sp"),
        ),
        check_vma=False,
    )
```

profile of v0, /device:TPU:24, one launch (start us, length us, event | category | flops | bytes accessed | tf_op | source)
XLA Modules:
  0.0 101.3 jit_solution(9303527365233248279)
XLA Ops:
  0.6 1.1 %copy.18 = bf16[1,768,64]{2,1,0:T(8,128)(2,1)S(1)} copy(bf16[1,768,64]{1,2,0:T(8,128)(2,1)} %param.16) | data formatting | bytes 196608 | tf_op args[3]
  1.7 0.0 copy-start.4
  1.7 0.9 copy-done.4
  2.6 0.0 copy-start.5
  2.6 0.9 copy-done.5
  3.5 16.3 %gather.1 = (bf16[8,64,1024]{2,1,0:T(8,128)(2,1)S(1)}, bf16[8,64,1024]{2,1,0:T(8,128)(2,1)S(1)}) custom-call(bf16[64,1024]{1,0:T(8,128)(2,1)S(1)} %copy-done.4, bf16[64,1024]{1,0:T(8,128)(2,1)S(1)} %copy-done.5), custom_call_target="tpu_custom_call" | custom-call | tf_op jit(solution)/shard_map/gather/pallas_call | solution.py:360
  19.8 0.0 copy-start.1
  19.8 1.1 %copy-done.1 = bf16[1,768,512]{2,1,0:T(8,128)(2,1)S(1)} copy-done((bf16[1,768,512]{2,1,0:T(8,128)(2,1)S(1)}, bf16[1,768,512]{2,1,0:T(8,128)(2,1)}, u32[]{:S(2)}) %copy-start.1) | copy-done | bytes 786456
  20.9 0.0 copy-start.2
  20.9 1.0 copy-done.2
  21.9 0.0 copy-start.3
  21.9 1.0 copy-done.3
  22.9 0.0 copy-start.6
  22.9 0.7 copy-done.6
  23.6 0.0 copy-start.7
  23.6 0.9 copy-done.7
  24.5 0.0 copy-start.8
  24.5 0.9 copy-done.8
  25.4 24.1 %attention_backward.1 = (bf16[768,1536]{1,0:T(8,128)(2,1)}, bf16[8,2,64,1024]{3,2,1,0:T(8,128)(2,1)}, bf16[768,640]{1,0:T(8,128)(2,1)S(1)}) custom-call(bf16[768,512]{1,0:T(8,128)(2,1)S(1)} %bitcast.16, bf16[768,64]{1,0:T(8,128)(2,1)S(1)} %bitcast.18, f32[1,512]{1,0:T(1,128)S(1)} %bitcast.19, f32[768,128]{1,0:T(8,128)S(1)} %copy-done.3, ...), custom_call_target="tpu_custom_call" | custom-call | flops 10000000000 | bytes 12000000 | tf_op jit(solution)/shard_map/attention_backward/pallas_call | solution.py:151
  49.5 0.0 copy-start
  49.5 1.6 %copy-done = bf16[8,2,64,1024]{3,2,1,0:T(8,128)(2,1)S(1)} copy-done((bf16[8,2,64,1024]{3,2,1,0:T(8,128)(2,1)S(1)}, bf16[8,2,64,1024]{3,2,1,0:T(8,128)(2,1)}, u32[]{:S(2)}) %copy-start) | copy-done | bytes 2097176
  51.1 47.6 %exchange.1 = (f32[2,64,1024]{2,1,0:T(8,128)S(1)}, bf16[768,640]{1,0:T(8,128)(2,1)S(1)}) custom-call(bf16[8,2,64,1024]{3,2,1,0:T(8,128)(2,1)S(1)} %copy-done, bf16[768,640]{1,0:T(8,128)(2,1)S(1)} %get-tuple-element.16.part_ref, bf16[768,512]{1,0:T(8,128)(2,1)S(1)} %bitcast.17, f32[1,512]{1,0:T(1,128)S(1)} %bitcast.20, f32[768,128]{1,0:T(8,128)S(1)} %copy-done.3, ...), custom_call_target="tpu_custom_call" | custom-call | tf_op jit(solution)/shard_map/exchange/pallas_call | solution.py:270
  98.8 0.8 slice_bitcast_fusion.1
  99.6 0.9 slice_bitcast_fusion
  100.6 0.8 copy.19
  (1 shorter events, 0.0 us)
Async XLA Ops:
  1.7 0.9 copy-start.4
  2.6 0.9 copy-start.5
  19.8 1.1 %copy-start.1 = (bf16[1,768,512]{2,1,0:T(8,128)(2,1)S(1)}, bf16[1,768,512]{2,1,0:T(8,128)(2,1)}, u32[]{:S(2)}) copy-start(bf16[1,768,512]{2,1,0:T(8,128)(2,1)} %param.15) | copy-start | bytes 2359300
  20.9 1.0 copy-start.2
  21.9 1.0 copy-start.3
  22.9 0.7 copy-start.6
  23.6 0.9 copy-start.7
  24.5 0.9 copy-start.8
  49.5 1.6 %copy-start = (bf16[8,2,64,1024]{3,2,1,0:T(8,128)(2,1)S(1)}, bf16[8,2,64,1024]{3,2,1,0:T(8,128)(2,1)}, u32[]{:S(2)}) copy-start(bf16[8,2,64,1024]{3,2,1,0:T(8,128)(2,1)} %get-tuple-element.15.dw_ref) | copy-start | bytes 6291460
where the time goes:
time: 102 us; the launch traced here: 101 us
  Pallas kernels  88 us (86%)
  local copies, waits for them, and re-layouts  12.6 us (12%)
    pallas_call x1, Pallas kernels, exchange(): pl.pallas_call(functools.partial(exchange_kernel, n_sp, n_dp), in_specs=[...  47.6 us
    pallas_call x1, Pallas kernels, attention(): pl.pallas_call(functools.partial(attention_kernel, block, grad_scale), gr...  24.1 us
    pallas_call x1, Pallas kernels, gather(): pl.pallas_call(functools.partial(gather_kernel, n_dp), in_specs=[vmem] *...  16.3 us
    unnamed x20, local copies, waits for them, and re-layouts  10.8 us

commit v1 on v0

v1 whole, which is shorter than its diff:
```python
import functools

import jax
import jax.numpy as jnp
import numpy as np
from jax import lax
from jax.experimental import pallas as pl
from jax.experimental.pallas import tpu as pltpu
from jax.sharding import PartitionSpec as P

NOPE_DIM = 128
ROPE_DIM = 64
VALUE_DIM = 128
QK = NOPE_DIM + ROPE_DIM
LOG2E = 1.4426950408889634

norm_eps = 1e-06
rope_theta = 10000.0

NT = (((1,), (1,)), ((), ()))
MESH = pl.DeviceIdType.MESH


def rope_tables(length):
    half = ROPE_DIM // 2
    frequency = np.float32(rope_theta) ** (-(np.arange(half, dtype=np.float32) * np.float32(2.0 / ROPE_DIM)))
    angles = np.arange(length, dtype=np.float32)[:, None] * frequency.astype(np.float32)[None, :]
    return np.cos(angles).astype(np.float32), np.sin(angles).astype(np.float32)


def dot(a, b):
    return jnp.dot(a, b, preferred_element_type=jnp.float32)


def dot_nt(a, b):
    return lax.dot_general(a, b, NT, preferred_element_type=jnp.float32)


def swap_halves(x):
    lane = lax.broadcasted_iota(jnp.int32, x.shape, 1)
    return jnp.where(lane % ROPE_DIM < ROPE_DIM // 2, pltpu.roll(x, 96, 1), pltpu.roll(x, 32, 1))


def each(first, count, act):
    def body(k, carry):
        act(k)
        return carry
    lax.fori_loop(first, count, body, 0)


def kernel(
    block, grad_scale, n_sp, n_dp,
    latent_hbm, rope_hbm, gain_hbm, cos_hbm, sin_hbm, cos_t_hbm, sin_t_hbm,
    q_hbm, do_hbm, wk_hbm, wv_hbm,
    dq_ref, grad_ref, low_ref,
    lat, rope, gain, cosw, sinw, cost, sint, qin, doin, w,
    comp, comp_t, krot, krot_t, ku, kt, vals, qu, pt, dst, dkv, acc, rot_acc,
    part, got_part, dwbuf, got_near, red, got_far,
    in_sem, w_sem, q_sem, do_sem,
    far_s, far_r, near_s, near_r, a_s, a_r, b_s, b_r, c_s, c_r, d_s, d_r,
):
    sp, dp = lax.axis_index("sp"), lax.axis_index("dp")
    chips = n_dp // 2
    chip, core = dp // 2, lax.rem(dp, 2)
    partner = chip * 2 + 1 - core
    pairs, length = qin.shape[0], qin.shape[1]
    width = lat.shape[1]
    tiles = length // block
    sub = block // n_sp
    scale = QK ** (-0.5)
    barrier = pltpu.get_barrier_semaphore()

    def chip_at(k):
        return lax.rem(chip + k, chips)

    def other(k):
        return chip_at(k) * 2 + core

    def source(k):
        return lax.rem(chip - k + chips, chips) * 2 + core

    def sp_peer(k):
        return lax.rem(sp + k, n_sp)

    def w_load(p, t):
        hbm = (wk_hbm, wv_hbm)[t]
        return pltpu.make_async_copy(
            hbm.at[:, pl.ds(pl.multiple_of(p * 256, 256), 256)],
            w.at[p, dp, :, pl.ds(t * 256, 256)], w_sem.at[p, t])

    for t in range(2):
        each(0, pairs, lambda p: w_load(p, t).start())
    each(1, chips, lambda k: pl.semaphore_signal(
        barrier, inc=1, device_id={"dp": other(k)}, device_id_type=MESH))
    each(1, n_sp, lambda k: pl.semaphore_signal(
        barrier, inc=1, device_id={"sp": sp_peer(k)}, device_id_type=MESH))
    pl.semaphore_signal(barrier, inc=1, device_id={"dp": partner}, device_id_type=MESH)

    loads = [
        pltpu.make_async_copy(src, dst_, in_sem.at[j]) for j, (src, dst_) in enumerate((
            (latent_hbm, lat), (gain_hbm, gain), (rope_hbm, rope), (cos_t_hbm, cost), (sin_t_hbm, sint),
            (cos_hbm, cosw), (sin_hbm, sinw)))]

    def q_load(p):
        return pltpu.make_async_copy(
            q_hbm.at[:, pl.ds(pl.multiple_of(p * 2 * QK, 128), 2 * QK)], qin.at[p], q_sem.at[p])

    def do_load(p):
        return pltpu.make_async_copy(
            do_hbm.at[:, pl.ds(pl.multiple_of(p * 256, 256), 256)], doin.at[p], do_sem.at[p])

    for copy in loads:
        copy.start()
    each(0, pairs, lambda p: q_load(p).start())
    each(0, pairs, lambda p: do_load(p).start())

    def far(p, k):
        return pltpu.make_async_remote_copy(
            src_ref=w.at[p, dp], dst_ref=w.at[p, dp],
            send_sem=far_s.at[p, k], recv_sem=far_r.at[p, k],
            device_id={"dp": other(k)}, device_id_type=MESH)

    def near(p, k):
        row = source(k)
        return pltpu.make_async_remote_copy(
            src_ref=w.at[p, row], dst_ref=w.at[p, row],
            send_sem=near_s.at[p, k], recv_sem=near_r.at[p, k],
            device_id={"dp": partner}, device_id_type=MESH)

    for t in range(2):
        each(0, pairs, lambda p: w_load(p, t).wait())
    pl.semaphore_wait(barrier, chips + n_sp - 1)

    def send_weights(p):
        each(1, chips, lambda k: far(p, k).start())
        near(p, 0).start()
    each(0, pairs, send_weights)

    def forward(p):
        def go(k):
            far(p, k).wait_recv()
            near(p, k).start()
        each(1, chips, go)

    for copy in loads:
        copy.wait()
    raw = lat[...].astype(jnp.float32)
    inverse = lax.rsqrt(jnp.mean(raw * raw, axis=-1, keepdims=True) + norm_eps)
    normed = raw * inverse * gain[...]
    comp[...] = normed.astype(jnp.bfloat16)
    comp_t[...] = normed.T.astype(jnp.bfloat16)
    ra = rope[:ROPE_DIM // 2, :].astype(jnp.float32)
    rb = rope[ROPE_DIM // 2:, :].astype(jnp.float32)
    turned = jnp.concatenate([ra * cost[...] - rb * sint[...], rb * cost[...] + ra * sint[...]], axis=0)
    krot_t[...] = turned.astype(jnp.bfloat16)
    krot[...] = jnp.concatenate([turned, turned], axis=0).T.astype(jnp.bfloat16)

    def turn_queries(p):
        q_load(p).wait()
        mid = qin[p, :, 128:256].astype(jnp.float32)
        last = qin[p, :, 256:384].astype(jnp.float32)
        low = lax.broadcasted_iota(jnp.int32, mid.shape, 1) < 64
        plain = jnp.where(low, pltpu.roll(mid, 64, 1), pltpu.roll(last, 64, 1))
        both = jnp.where(low, mid, last)
        rot = both * cosw[...] + swap_halves(both) * sinw[...]
        qu[2 * p, :, :NOPE_DIM] = qin[p, :, :128]
        qu[2 * p, :, NOPE_DIM:] = rot[:, :ROPE_DIM].astype(jnp.bfloat16)
        qu[2 * p + 1, :, :NOPE_DIM] = plain.astype(jnp.bfloat16)
        qu[2 * p + 1, :, NOPE_DIM:] = pltpu.roll(rot, 64, 1)[:, :ROPE_DIM].astype(jnp.bfloat16)
    each(0, pairs, turn_queries)
    each(0, pairs, lambda p: do_load(p).wait())

    def project(p):
        each(0, chips, lambda k: near(p, k).wait_recv())
        both = dot(comp[...], w[p].reshape(width, 512))
        keys = both[:, :256]
        keys_t = keys.T.astype(jnp.bfloat16)
        keys = keys.astype(jnp.bfloat16)
        vals[p] = both[:, 256:].astype(jnp.bfloat16)
        for h in range(2):
            ku[2 * p + h, :, :NOPE_DIM] = keys[:, h * NOPE_DIM:(h + 1) * NOPE_DIM]
            ku[2 * p + h, :, NOPE_DIM:] = krot[:, :ROPE_DIM]
            kt[2 * p + h, :NOPE_DIM, :] = keys_t[h * NOPE_DIM:(h + 1) * NOPE_DIM, :]
            kt[2 * p + h, NOPE_DIM:, :] = krot_t[...]

    def attend(i, p):
        rows = slice(i * block, (i + 1) * block)
        n = (i + 1) * block
        for h in range(2):
            cols = slice(h * VALUE_DIM, (h + 1) * VALUE_DIM)
            scores = dot_nt(ku[2 * p + h, :n, :], qu[2 * p + h, rows, :])
            key_at = lax.broadcasted_iota(jnp.int32, (block, block), 0)
            query_at = lax.broadcasted_iota(jnp.int32, (block, block), 1)
            diag = jnp.where(key_at <= query_at, scores[n - block:], -jnp.inf)
            scores = diag if i == 0 else jnp.concatenate([scores[:n - block], diag], axis=0)
            top = jnp.max(scores, axis=0, keepdims=True)
            e = jnp.exp2((scores - top) * (scale * LOG2E))
            r = 1.0 / jnp.sum(e, axis=0, keepdims=True)
            prob_grad = dot_nt(vals[p, :n, cols], doin[p, rows, cols])
            center = jnp.sum(e * prob_grad, axis=0, keepdims=True) * r
            pt[2 * p + h, :n, rows] = (e * r).astype(jnp.bfloat16)
            dst[2 * p + h, :n, rows] = (e * (r * scale) * (prob_grad - center)).astype(jnp.bfloat16)

    def key_block(i, p):
        rows = slice(i * block, (i + 1) * block)
        rot = None
        for h in range(2):
            cols = slice(h * VALUE_DIM, (h + 1) * VALUE_DIM)
            dv = dot(pt[2 * p + h, rows, i * block:], doin[p, i * block:, cols])
            dk = dot(dst[2 * p + h, rows, i * block:], qu[2 * p + h, i * block:, :])
            dkv[p, rows, h * NOPE_DIM:(h + 1) * NOPE_DIM] = dk[:, :NOPE_DIM].astype(jnp.bfloat16)
            dkv[p, rows, (2 + h) * 128:(3 + h) * 128] = dv.astype(jnp.bfloat16)
            rot = dk[:, NOPE_DIM:] if rot is None else rot + dk[:, NOPE_DIM:]
        rot_acc[...] += rot
        acc[...] += dot_nt(dkv[p, rows, :], w[p].reshape(width, 512))

    def part_copy(i, k):
        peer = sp_peer(k)
        return pltpu.make_async_remote_copy(
            src_ref=part.at[i, peer], dst_ref=got_part.at[i, k],
            send_sem=a_s.at[i, k], recv_sem=a_r.at[i, k],
            device_id={"sp": peer}, device_id_type=MESH)

    def low_copy(i, k):
        return pltpu.make_async_remote_copy(
            src_ref=low_ref.at[i, sp], dst_ref=low_ref.at[i, sp],
            send_sem=b_s.at[i, k], recv_sem=b_r.at[i, k],
            device_id={"sp": sp_peer(k)}, device_id_type=MESH)

    def send_part(i):
        rot = rot_acc[...].astype(jnp.bfloat16)
        whole = jnp.concatenate([acc[...].astype(jnp.bfloat16), rot, rot], axis=1)
        part[i] = whole.reshape(n_sp, sub, width + 128)
        each(1, n_sp, lambda k: part_copy(i, k).start())

    def finish(i):
        each(1, n_sp, lambda k: part_copy(i, k).wait())
        total = part[i, sp].astype(jnp.float32)
        for k in range(1, n_sp):
            total = total + got_part[i, k].astype(jnp.float32)
        mine = pl.ds(pl.multiple_of(i * block + sp * sub, sub), sub)
        raw = lat[mine, :].astype(jnp.float32)
        inverse = lax.rsqrt(jnp.mean(raw * raw, axis=-1, keepdims=True) + norm_eps)
        mixed = total[:, :width] * gain[...]
        spread = jnp.mean(raw * mixed, axis=-1, keepdims=True)
        low_ref[i, sp, :, :width] = (inverse * mixed - raw * inverse**3 * spread).astype(jnp.bfloat16)
        rot = total[:, width:]
        low_ref[i, sp, :, width:] = (
            rot * cosw[mine, :] - swap_halves(rot) * sinw[mine, :]
        ).astype(jnp.bfloat16)
        each(1, n_sp, lambda k: low_copy(i, k).start())

    def near_grad(p):
        return pltpu.make_async_remote_copy(
            src_ref=dwbuf.at[p, 1 - core], dst_ref=got_near.at[p],
            send_sem=c_s.at[p], recv_sem=c_r.at[p],
            device_id={"dp": partner}, device_id_type=MESH)

    def far_grad(p, k):
        return pltpu.make_async_remote_copy(
            src_ref=red.at[p, chip_at(k)], dst_ref=got_far.at[p, k],
            send_sem=d_s.at[p, k], recv_sem=d_r.at[p, k],
            device_id={"dp": other(k)}, device_id_type=MESH)

    def weight_grad(p):
        dw = dot(comp_t[...], dkv[p]) * grad_scale
        dw = dw.reshape(chips, 2, width // n_dp, 512)
        for c in range(2):
            dwbuf[p, c] = dw[:, c].astype(jnp.bfloat16)
        near_grad(p).start()

    def chip_grad(p):
        near_grad(p).wait_recv()
        both = dwbuf[p, core].astype(jnp.float32) + got_near[p].astype(jnp.float32)
        red[p] = both.astype(jnp.bfloat16)
        each(1, chips, lambda k: far_grad(p, k).start())

    def query_grad(i, p):
        rows = slice(i * block, (i + 1) * block)
        n = (i + 1) * block
        parts = []
        for h in range(2):
            g = dot(kt[2 * p + h, :, :n], dst[2 * p + h, :n, rows])
            a = g[NOPE_DIM:NOPE_DIM + 32]
            b = g[NOPE_DIM + 32:]
            c, s = cost[:, rows], sint[:, rows]
            parts += [g[:NOPE_DIM], a * c + b * s, b * c - a * s]
        dq_ref[rows, pl.ds(pl.multiple_of(p * 2 * QK, 128), 2 * QK)] = (
            jnp.concatenate(parts, axis=0).T.astype(jnp.bfloat16))

    forward(0)
    for i in reversed(range(tiles)):
        acc[...] = jnp.zeros_like(acc)
        rot_acc[...] = jnp.zeros_like(rot_acc)

        def step(p, i=i):
            if i == tiles - 1:
                project(p)
            attend(i, p)
            if i == tiles - 1:
                pl.when(p + 1 < pairs)(lambda: forward(p + 1))
            key_block(i, p)
        each(0, pairs, step)
        send_part(i)

    finish(tiles - 1)

    def grads(p):
        weight_grad(p)
        pl.when(p > 0)(lambda: chip_grad(p - 1))
    each(0, pairs, grads)
    chip_grad(pairs - 1)
    for i in range(tiles - 2, 0, -1):
        finish(i)

    for i in reversed(range(tiles)):
        each(0, pairs, lambda p, i=i: query_grad(i, p))

    if tiles > 1:
        finish(0)

    def add(p):
        total = red[p, chip].astype(jnp.float32)
        for k in range(1, chips):
            far_grad(p, k).wait()
            total = total + got_far[p, k].astype(jnp.float32)
        cols = pl.ds(pl.multiple_of(p * 256, 256), 256)
        grad_ref[0, :, cols] = total[:, :256]
        grad_ref[1, :, cols] = total[:, 256:]
        near_grad(p).wait_send()
        def drain(k):
            far(p, k).wait_send()
            near(p, k).wait_send()
        each(1, chips, drain)
        near(p, 0).wait_send()
    each(0, pairs, add)
    for i in range(tiles):
        each(1, n_sp, lambda k: low_copy(i, k).wait())


def fused(queries, out_grad, latent, rope_t, kv_gain, key_up, value_up, grad_scale, n_sp, n_dp):
    length, width = latent.shape
    pairs = key_up.shape[1] // 256
    heads = 2 * pairs
    chips = n_dp // 2
    block = 256
    tiles = length // block
    sub = block // n_sp
    depth = key_up.shape[0]
    cosine, sine = rope_tables(length)
    bf, f32 = jnp.bfloat16, jnp.float32
    hbm = pl.BlockSpec(memory_space=pl.ANY)
    vmem = pl.BlockSpec(memory_space=pltpu.VMEM)
    dma = lambda *n: pltpu.SemaphoreType.DMA(n)
    V = pltpu.VMEM
    return pl.pallas_call(
        functools.partial(kernel, block, grad_scale, n_sp, n_dp),
        in_specs=[hbm] * 11,
        out_specs=[vmem] * 3,
        out_shape=[
            jax.ShapeDtypeStruct(queries.shape, bf),
            jax.ShapeDtypeStruct((2, *key_up.shape), f32),
            jax.ShapeDtypeStruct((tiles, n_sp, sub, width + 128), bf),
        ],
        scratch_shapes=[
            V((length, width), bf), V((ROPE_DIM, length), bf), V((1, width), f32),
            V((length, 128), f32), V((length, 128), f32), V((32, length), f32), V((32, length), f32),
            V((pairs, length, 2 * QK), bf), V((pairs, length, 256), bf), V((pairs, n_dp, depth, 512), bf),
            V((length, width), bf), V((width, length), bf), V((length, 128), bf), V((ROPE_DIM, length), bf),
            V((heads, length, QK), bf), V((heads, QK, length), bf), V((pairs, length, 256), bf),
            V((heads, length, QK), bf), V((heads, length, length), bf), V((heads, length, length), bf),
            V((pairs, length, 512), bf), V((block, width), f32), V((block, ROPE_DIM), f32),
            V((tiles, n_sp, sub, width + 128), bf), V((tiles, n_sp, sub, width + 128), bf),
            V((pairs, 2, chips, depth, 512), bf), V((pairs, chips, depth, 512), bf),
            V((pairs, chips, depth, 512), bf), V((pairs, chips, depth, 512), bf),
            dma(7), dma(pairs, 2), dma(pairs), dma(pairs),
            dma(pairs, chips), dma(pairs, chips), dma(pairs, chips), dma(pairs, chips),
            dma(tiles, n_sp), dma(tiles, n_sp), dma(tiles, n_sp), dma(tiles, n_sp),
            dma(pairs), dma(pairs), dma(pairs, chips), dma(pairs, chips),
        ],
        compiler_params=pltpu.CompilerParams(
            collective_id=0, has_side_effects=True, vmem_limit_bytes=62 * 1024 * 1024
        ),
        name="fused_backward",
    )(
        latent, rope_t, kv_gain.reshape(1, -1), np.tile(cosine, (1, 4)),
        np.concatenate([-sine, sine, -sine, sine], axis=1),
        np.ascontiguousarray(cosine.T), np.ascontiguousarray(sine.T),
        queries, out_grad, key_up, value_up,
    )


def write_kernel(dq_ref, grad_ref, low_ref, dq_out, lat_out, rot_out, key_out, value_out, rot, sem):
    width = lat_out.shape[1]
    copies = [
        pltpu.make_async_copy(src, dst_, sem.at[j]) for j, (src, dst_) in enumerate((
            (dq_ref, dq_out), (low_ref.at[:, pl.ds(0, width)], lat_out),
            (grad_ref.at[0], key_out), (grad_ref.at[1], value_out), (rot, rot_out)))]
    for copy in copies[:4]:
        copy.start()
    rot[...] = low_ref[:, width:].astype(jnp.float32).T[:ROPE_DIM].astype(jnp.bfloat16)
    copies[4].start()
    for copy in copies:
        copy.wait()


def write(dq, grad, low):
    length, width = low.shape[0], low.shape[1] - 128
    bf, f32 = jnp.bfloat16, jnp.float32
    return pl.pallas_call(
        write_kernel,
        in_specs=[pl.BlockSpec(memory_space=pltpu.VMEM)] * 3,
        out_specs=[pl.BlockSpec(memory_space=pl.ANY)] * 5,
        out_shape=[
            jax.ShapeDtypeStruct(dq.shape, bf),
            jax.ShapeDtypeStruct((length, width), bf),
            jax.ShapeDtypeStruct((ROPE_DIM, length), bf),
            jax.ShapeDtypeStruct(grad.shape[1:], f32),
            jax.ShapeDtypeStruct(grad.shape[1:], f32),
        ],
        scratch_shapes=[pltpu.VMEM((ROPE_DIM, length), bf), pltpu.SemaphoreType.DMA((5,))],
        compiler_params=pltpu.CompilerParams(vmem_limit_bytes=16 * 1024 * 1024),
        name="write_outputs",
    )(dq, grad, low)


def shards(queries, out_grad, latent, rope_key, kv_gain, key_up, value_up):
    length, width = latent.shape[1:]
    n_sp, n_dp = lax.axis_size("sp"), lax.axis_size("dp")
    grad_scale = float(n_dp * length) ** (-0.5)
    rope_t = jnp.swapaxes(rope_key, 1, 2)[0]
    dq, grad, low = fused(
        queries[0], out_grad[0], latent[0], rope_t, kv_gain, key_up, value_up, grad_scale, n_sp, n_dp
    )
    dq, lat, rot_t, key_grad, value_grad = write(dq, grad, low.reshape(length, width + 128))
    return dq[None], lat[None], jnp.swapaxes(rot_t[None], 1, 2), key_grad, value_grad


def solution(mesh):
    return jax.shard_map(
        shards,
        mesh=mesh,
        in_specs=(
            P("dp", None, "sp"),
            P("dp", None, "sp"),
            P("dp", None, None),
            P("dp", None, None),
            P(),
            P("dp", "sp"),
            P("dp", "sp"),
        ),
        out_specs=(
            P("dp", None, "sp"),
            P("dp", None, None),
            P("dp", None, None),
            P("dp", "sp"),
            P("dp", "sp"),
        ),
        check_vma=False,
    )
```

time: 102 us -> 76.8 us (0.75)
  the two profiles are of different devices: /device:TPU:24 before, /device:TPU:0 now
where the time goes in v1:
time: 76.8 us; the launch traced here: 76.5 us
  Pallas kernels  72 us (94%)
  local copies, waits for them, and re-layouts  3.9 us (5%)
    pallas_call x1, Pallas kernels, fused(): pl.pallas_call(functools.partial(kernel, block, grad_scale, n_sp, n_dp),...  70.1 us
    unnamed x6, local copies, waits for them, and re-layouts  3.9 us
    pallas_call x1, Pallas kernels, write(): pl.pallas_call(write_kernel, in_specs=[pl.BlockSpec(memory_space=pltpu.VM...  1.89 us

profile of v1, /device:TPU:0, one launch (start us, length us, event | category | flops | bytes accessed | tf_op | source)
XLA Modules:
  0.0 76.5 jit_solution(377626014936719044)
XLA Ops:
  0.6 70.1 %fused_backward.1 = (bf16[768,1536]{1,0:T(8,128)(2,1)}, f32[2,64,1024]{2,1,0:T(8,128)}, bf16[3,4,64,640]{3,2,1,0:T(8,128)(2,1)}) custom-call(bf16[768,512]{1,0:T(8,128)(2,1)} %bitcast.16, bf16[64,768]{1,0:T(8,128)(2,1)} %bitcast.17, f32[1,512]{1,0:T(1,128)} %bitcast.18, f32[768,128]{1,0:T(8,128)} %constant.8.clone.cos_hbm, ...), custom_call_target="tpu_custom_call" | custom-call | tf_op jit(solution)/shard_map/fused_backward/pallas_call | solution.py:356
  70.7 0.0 copy-start
  70.7 1.7 %copy-done = bf16[768,1536]{1,0:T(8,128)(2,1)S(1)} copy-done((bf16[768,1536]{1,0:T(8,128)(2,1)S(1)}, bf16[768,1536]{1,0:T(8,128)(2,1)}, u32[]{:S(2)}) %copy-start) | copy-done | bytes 2359320
  72.4 0.0 copy-start.1
  72.4 1.2 %copy-done.1 = bf16[3,4,64,640]{3,2,1,0:T(8,128)(2,1)S(1)} copy-done((bf16[3,4,64,640]{3,2,1,0:T(8,128)(2,1)S(1)}, bf16[3,4,64,640]{3,2,1,0:T(8,128)(2,1)}, u32[]{:S(2)}) %copy-start.1) | copy-done | bytes 983064
  73.6 0.0 copy-start.2
  73.6 1.0 %copy-done.2 = f32[2,64,1024]{2,1,0:T(8,128)S(1)} copy-done((f32[2,64,1024]{2,1,0:T(8,128)S(1)}, f32[2,64,1024]{2,1,0:T(8,128)}, u32[]{:S(2)}) %copy-start.2) | copy-done | bytes 524312
  74.6 1.9 %write_outputs.1 = (bf16[768,1536]{1,0:T(8,128)(2,1)}, bf16[768,512]{1,0:T(8,128)(2,1)}, bf16[64,768]{1,0:T(8,128)(2,1)}, f32[64,1024]{1,0:T(8,128)}, f32[64,1024]{1,0:T(8,128)}) custom-call(bf16[768,1536]{1,0:T(8,128)(2,1)S(1)} %copy-done, f32[2,64,1024]{2,1,0:T(8,128)S(1)} %copy-done.2, bf16[768,640]{1,0:T(8,128)(2,1)S(1)} %bitcast.13), custom_call_target="tpu_custom_call" | custom-call | tf_op jit(solution)/shard_map/write_outputs/pallas_call | solution.py:410
Async XLA Ops:
  70.7 1.7 %copy-start = (bf16[768,1536]{1,0:T(8,128)(2,1)S(1)}, bf16[768,1536]{1,0:T(8,128)(2,1)}, u32[]{:S(2)}) copy-start(bf16[768,1536]{1,0:T(8,128)(2,1)} %get-tuple-element.13.dq_ref) | copy-start | bytes 7077892
  72.4 1.2 %copy-start.1 = (bf16[3,4,64,640]{3,2,1,0:T(8,128)(2,1)S(1)}, bf16[3,4,64,640]{3,2,1,0:T(8,128)(2,1)}, u32[]{:S(2)}) copy-start(bf16[3,4,64,640]{3,2,1,0:T(8,128)(2,1)} %get-tuple-element.15) | copy-start | bytes 2949124
  73.6 1.0 %copy-start.2 = (f32[2,64,1024]{2,1,0:T(8,128)S(1)}, f32[2,64,1024]{2,1,0:T(8,128)}, u32[]{:S(2)}) copy-start(f32[2,64,1024]{2,1,0:T(8,128)} %get-tuple-element.14.grad_ref) | copy-start | bytes 1572868

commit v2 on v1

--- a/solution.py
+++ b/solution.py
@@ -55,9 +55,9 @@
     dq_ref, grad_ref, low_ref,
     lat, rope, gain, cosw, sinw, cost, sint, qin, doin, w,
     comp, comp_t, krot, krot_t, ku, kt, vals, qu, pt, dst, dkv, acc, rot_acc,
-    part, got_part, dwbuf, got_near, red, got_far,
+    part, got_in, got_mid, dwbuf, got_near, red, got_far,
     in_sem, w_sem, q_sem, do_sem,
-    far_s, far_r, near_s, near_r, a_s, a_r, b_s, b_r, c_s, c_r, d_s, d_r,
+    far_s, far_r, near_s, near_r, a_s, a_r, m_s, m_r, b_s, b_r, c_s, c_r, d_s, d_r,
 ):
     sp, dp = lax.axis_index("sp"), lax.axis_index("dp")
     chips = n_dp // 2
@@ -66,7 +66,8 @@
     pairs, length = qin.shape[0], qin.shape[1]
     width = lat.shape[1]
     tiles = length // block
-    sub = block // n_sp
+    pieces = part.shape[1]
+    rows_of = block // pieces
     scale = QK ** (-0.5)
     barrier = pltpu.get_barrier_semaphore()
 
@@ -78,9 +79,6 @@
 
     def source(k):
         return lax.rem(chip - k + chips, chips) * 2 + core
-
-    def sp_peer(k):
-        return lax.rem(sp + k, n_sp)
 
     def w_load(p, t):
         hbm = (wk_hbm, wv_hbm)[t]
@@ -92,8 +90,14 @@
         each(0, pairs, lambda p: w_load(p, t).start())
     each(1, chips, lambda k: pl.semaphore_signal(
         barrier, inc=1, device_id={"dp": other(k)}, device_id_type=MESH))
-    each(1, n_sp, lambda k: pl.semaphore_signal(
-        barrier, inc=1, device_id={"sp": sp_peer(k)}, device_id_type=MESH))
+    lower = sp < n_sp // 2
+    at_end = jnp.logical_or(sp == 0, sp == n_sp - 1)
+    at_middle = jnp.logical_or(sp == n_sp // 2 - 1, sp == n_sp // 2)
+    inward = jnp.where(lower, sp + 1, sp - 1)
+    outward = jnp.where(lower, sp - 1, sp + 1)
+    pl.semaphore_signal(barrier, inc=1, device_id={"sp": inward}, device_id_type=MESH)
+    pl.when(jnp.logical_not(at_end))(lambda: pl.semaphore_signal(
+        barrier, inc=1, device_id={"sp": outward}, device_id_type=MESH))
     pl.semaphore_signal(barrier, inc=1, device_id={"dp": partner}, device_id_type=MESH)
 
     loads = [
@@ -129,7 +133,7 @@
 
     for t in range(2):
         each(0, pairs, lambda p: w_load(p, t).wait())
-    pl.semaphore_wait(barrier, chips + n_sp - 1)
+    pl.semaphore_wait(barrier, chips + jnp.where(at_end, 1, 2))
 
     def send_weights(p):
         each(1, chips, lambda k: far(p, k).start())
@@ -198,57 +202,91 @@
             r = 1.0 / jnp.sum(e, axis=0, keepdims=True)
             prob_grad = dot_nt(vals[p, :n, cols], doin[p, rows, cols])
             center = jnp.sum(e * prob_grad, axis=0, keepdims=True) * r
-            pt[2 * p + h, :n, rows] = (e * r).astype(jnp.bfloat16)
-            dst[2 * p + h, :n, rows] = (e * (r * scale) * (prob_grad - center)).astype(jnp.bfloat16)
+            prob = (e * r).astype(jnp.bfloat16)
+            grad = (e * (r * scale) * (prob_grad - center)).astype(jnp.bfloat16)
+            for j in range(i + 1):
+                at = slice((i - j) * block, (i - j + 1) * block)
+                pt[j][2 * p + h, :, at] = prob[j * block:(j + 1) * block]
+                dst[j][2 * p + h, :, at] = grad[j * block:(j + 1) * block]
 
     def key_block(i, p):
         rows = slice(i * block, (i + 1) * block)
         rot = None
         for h in range(2):
             cols = slice(h * VALUE_DIM, (h + 1) * VALUE_DIM)
-            dv = dot(pt[2 * p + h, rows, i * block:], doin[p, i * block:, cols])
-            dk = dot(dst[2 * p + h, rows, i * block:], qu[2 * p + h, i * block:, :])
+            dv = dot(pt[i][2 * p + h], doin[p, i * block:, cols])
+            dk = dot(dst[i][2 * p + h], qu[2 * p + h, i * block:, :])
             dkv[p, rows, h * NOPE_DIM:(h + 1) * NOPE_DIM] = dk[:, :NOPE_DIM].astype(jnp.bfloat16)
             dkv[p, rows, (2 + h) * 128:(3 + h) * 128] = dv.astype(jnp.bfloat16)
             rot = dk[:, NOPE_DIM:] if rot is None else rot + dk[:, NOPE_DIM:]
         rot_acc[...] += rot
         acc[...] += dot_nt(dkv[p, rows, :], w[p].reshape(width, 512))
 
-    def part_copy(i, k):
-        peer = sp_peer(k)
-        return pltpu.make_async_remote_copy(
-            src_ref=part.at[i, peer], dst_ref=got_part.at[i, k],
-            send_sem=a_s.at[i, k], recv_sem=a_r.at[i, k],
-            device_id={"sp": peer}, device_id_type=MESH)
-
-    def low_copy(i, k):
-        return pltpu.make_async_remote_copy(
-            src_ref=low_ref.at[i, sp], dst_ref=low_ref.at[i, sp],
-            send_sem=b_s.at[i, k], recv_sem=b_r.at[i, k],
-            device_id={"sp": sp_peer(k)}, device_id_type=MESH)
+    def in_copy(i, q):
+        return pltpu.make_async_remote_copy(
+            src_ref=part.at[i, q], dst_ref=got_in.at[i, q],
+            send_sem=a_s.at[i, q], recv_sem=a_r.at[i, q],
+            device_id={"sp": inward}, device_id_type=MESH)
+
+    def mid_copy(i, q):
+        return pltpu.make_async_remote_copy(
+            src_ref=part.at[i, q], dst_ref=got_mid.at[i, q],
+            send_sem=m_s.at[i, q], recv_sem=m_r.at[i, q],
+            device_id={"sp": inward}, device_id_type=MESH)
+
+    def out_copy(i, q):
+        return pltpu.make_async_remote_copy(
+            src_ref=low_ref.at[i, q], dst_ref=low_ref.at[i, q],
+            send_sem=b_s.at[i, q], recv_sem=b_r.at[i, q],
+            device_id={"sp": outward}, device_id_type=MESH)
+
+    def go_in(i, q):
+        pl.when(at_middle)(lambda: mid_copy(i, q).start())
+        pl.when(jnp.logical_not(at_middle))(lambda: in_copy(i, q).start())
 
     def send_part(i):
         rot = rot_acc[...].astype(jnp.bfloat16)
         whole = jnp.concatenate([acc[...].astype(jnp.bfloat16), rot, rot], axis=1)
-        part[i] = whole.reshape(n_sp, sub, width + 128)
-        each(1, n_sp, lambda k: part_copy(i, k).start())
-
-    def finish(i):
-        each(1, n_sp, lambda k: part_copy(i, k).wait())
-        total = part[i, sp].astype(jnp.float32)
-        for k in range(1, n_sp):
-            total = total + got_part[i, k].astype(jnp.float32)
-        mine = pl.ds(pl.multiple_of(i * block + sp * sub, sub), sub)
-        raw = lat[mine, :].astype(jnp.float32)
-        inverse = lax.rsqrt(jnp.mean(raw * raw, axis=-1, keepdims=True) + norm_eps)
-        mixed = total[:, :width] * gain[...]
-        spread = jnp.mean(raw * mixed, axis=-1, keepdims=True)
-        low_ref[i, sp, :, :width] = (inverse * mixed - raw * inverse**3 * spread).astype(jnp.bfloat16)
-        rot = total[:, width:]
-        low_ref[i, sp, :, width:] = (
-            rot * cosw[mine, :] - swap_halves(rot) * sinw[mine, :]
-        ).astype(jnp.bfloat16)
-        each(1, n_sp, lambda k: low_copy(i, k).start())
+        part[i] = whole.reshape(pieces, rows_of, width + 128)
+        def go():
+            for q in range(pieces):
+                go_in(i, q)
+        pl.when(at_end)(go)
+
+    def merge(i, q):
+        def go():
+            in_copy(i, q).wait_recv()
+            part[i, q] = (part[i, q].astype(jnp.float32) + got_in[i, q].astype(jnp.float32)).astype(jnp.bfloat16)
+            go_in(i, q)
+        pl.when(jnp.logical_not(at_end))(go)
+
+    def finish(i, q):
+        def go():
+            mid_copy(i, q).wait_recv()
+            total = part[i, q].astype(jnp.float32) + got_mid[i, q].astype(jnp.float32)
+            mine = slice(i * block + q * rows_of, i * block + (q + 1) * rows_of)
+            raw = lat[mine, :].astype(jnp.float32)
+            inverse = lax.rsqrt(jnp.mean(raw * raw, axis=-1, keepdims=True) + norm_eps)
+            mixed = total[:, :width] * gain[...]
+            spread = jnp.mean(raw * mixed, axis=-1, keepdims=True)
+            low_ref[i, q, :, :width] = (inverse * mixed - raw * inverse**3 * spread).astype(jnp.bfloat16)
+            rot = total[:, width:]
+            low_ref[i, q, :, width:] = (
+                rot * cosw[mine, :] - swap_halves(rot) * sinw[mine, :]
+            ).astype(jnp.bfloat16)
+            pl.when(jnp.logical_not(at_end))(lambda: out_copy(i, q).start())
+        pl.when(at_middle)(go)
+
+    def deliver(i, q):
+        def go():
+            out_copy(i, q).wait_recv()
+            pl.when(jnp.logical_not(at_end))(lambda: out_copy(i, q).start())
+        pl.when(jnp.logical_not(at_middle))(go)
+
+    def drain_rows(i, q):
+        pl.when(at_middle)(lambda: mid_copy(i, q).wait_send())
+        pl.when(jnp.logical_not(at_middle))(lambda: in_copy(i, q).wait_send())
+        pl.when(jnp.logical_not(at_end))(lambda: out_copy(i, q).wait_send())
 
     def near_grad(p):
         return pltpu.make_async_remote_copy(
@@ -280,13 +318,42 @@
         n = (i + 1) * block
         parts = []
         for h in range(2):
-            g = dot(kt[2 * p + h, :, :n], dst[2 * p + h, :n, rows])
+            g = dot(kt[2 * p + h, :, :n], jnp.concatenate(
+                [dst[j][2 * p + h, :, (i - j) * block:(i - j + 1) * block] for j in range(i + 1)], axis=0))
             a = g[NOPE_DIM:NOPE_DIM + 32]
             b = g[NOPE_DIM + 32:]
             c, s = cost[:, rows], sint[:, rows]
             parts += [g[:NOPE_DIM], a * c + b * s, b * c - a * s]
         dq_ref[rows, pl.ds(pl.multiple_of(p * 2 * QK, 128), 2 * QK)] = (
             jnp.concatenate(parts, axis=0).T.astype(jnp.bfloat16))
+
+    last = pairs - 1
+    stages = {}
+
+    def stage(act, i, *keys):
+        for q, key in enumerate(keys):
+            phase, at = key if isinstance(key, tuple) else (key, None)
+            key = phase if at is None else (phase, min(at, last))
+            stages.setdefault(key, []).append(functools.partial(act, i, q))
+
+    for i in range(tiles - 1, 0, -1):
+        if i > 1:
+            stage(merge, i, (i - 1, 2), (i - 1, 3), ("sent", i - 1), (i - 2, 0))
+            stage(finish, i, (i - 2, 0), (i - 2, 1), (i - 2, 2), (i - 2, 3))
+        else:
+            stage(merge, 1, (0, 2), (0, 3), ("w", 1), ("w", 3))
+            stage(finish, 1, ("w", 3), "grads", ("q2", 2), ("q1", 1))
+    stage(merge, 0, ("q2", 2), ("q1", 2), "end", "end3")
+    stage(finish, 0, "end1", "end4", "end5", "end6")
+
+    def run(key):
+        for act in stages.pop(key, []):
+            act()
+
+    def run_in(name, p):
+        for at in range(pairs):
+            if (name, at) in stages:
+                pl.when(p == at)(functools.partial(run, (name, at)))
 
     forward(0)
     for i in reversed(range(tiles)):
@@ -300,24 +367,27 @@
             if i == tiles - 1:
                 pl.when(p + 1 < pairs)(lambda: forward(p + 1))
             key_block(i, p)
+            run_in(i, p)
         each(0, pairs, step)
         send_part(i)
-
-    finish(tiles - 1)
+        run(("sent", min(i, last)))
 
     def grads(p):
         weight_grad(p)
         pl.when(p > 0)(lambda: chip_grad(p - 1))
+        run_in("w", p)
     each(0, pairs, grads)
     chip_grad(pairs - 1)
-    for i in range(tiles - 2, 0, -1):
-        finish(i)
+    run("grads")
 
     for i in reversed(range(tiles)):
-        each(0, pairs, lambda p, i=i: query_grad(i, p))
-
-    if tiles > 1:
-        finish(0)
+        def turn_back(p, i=i):
+            query_grad(i, p)
+            run_in("q" + str(i), p)
+        each(0, pairs, turn_back)
+    for key in sorted(k for k in stages if isinstance(k, str)):
+        run(key)
+    assert not stages
 
     def add(p):
         total = red[p, chip].astype(jnp.float32)
@@ -334,8 +404,10 @@
         each(1, chips, drain)
         near(p, 0).wait_send()
     each(0, pairs, add)
-    for i in range(tiles):
-        each(1, n_sp, lambda k: low_copy(i, k).wait())
+    for i in reversed(range(tiles)):
+        for q in range(pieces):
+            deliver(i, q)
+            drain_rows(i, q)
 
 
 def fused(queries, out_grad, latent, rope_t, kv_gain, key_up, value_up, grad_scale, n_sp, n_dp):
@@ -345,14 +417,16 @@
     chips = n_dp // 2
     block = 256
     tiles = length // block
-    sub = block // n_sp
+    pieces = 4
+    piece = (tiles, pieces, block // pieces, width + 128)
     depth = key_up.shape[0]
     cosine, sine = rope_tables(length)
     bf, f32 = jnp.bfloat16, jnp.float32
-    hbm = pl.BlockSpec(memory_space=pl.ANY)
+    hbm = pl.BlockSpec(memory_space=pltpu.HBM)
     vmem = pl.BlockSpec(memory_space=pltpu.VMEM)
     dma = lambda *n: pltpu.SemaphoreType.DMA(n)
     V = pltpu.VMEM
+    triangle = tuple(V((heads, block, length - j * block), bf) for j in range(tiles))
     return pl.pallas_call(
         functools.partial(kernel, block, grad_scale, n_sp, n_dp),
         in_specs=[hbm] * 11,
@@ -360,7 +434,7 @@
         out_shape=[
             jax.ShapeDtypeStruct(queries.shape, bf),
             jax.ShapeDtypeStruct((2, *key_up.shape), f32),
-            jax.ShapeDtypeStruct((tiles, n_sp, sub, width + 128), bf),
+            jax.ShapeDtypeStruct(piece, bf),
         ],
         scratch_shapes=[
             V((length, width), bf), V((ROPE_DIM, length), bf), V((1, width), f32),
@@ -368,26 +442,26 @@
             V((pairs, length, 2 * QK), bf), V((pairs, length, 256), bf), V((pairs, n_dp, depth, 512), bf),
             V((length, width), bf), V((width, length), bf), V((length, 128), bf), V((ROPE_DIM, length), bf),
             V((heads, length, QK), bf), V((heads, QK, length), bf), V((pairs, length, 256), bf),
-            V((heads, length, QK), bf), V((heads, length, length), bf), V((heads, length, length), bf),
+            V((heads, length, QK), bf), triangle, triangle,
             V((pairs, length, 512), bf), V((block, width), f32), V((block, ROPE_DIM), f32),
-            V((tiles, n_sp, sub, width + 128), bf), V((tiles, n_sp, sub, width + 128), bf),
+            V(piece, bf), V(piece, bf), V(piece, bf),
             V((pairs, 2, chips, depth, 512), bf), V((pairs, chips, depth, 512), bf),
             V((pairs, chips, depth, 512), bf), V((pairs, chips, depth, 512), bf),
             dma(7), dma(pairs, 2), dma(pairs), dma(pairs),
             dma(pairs, chips), dma(pairs, chips), dma(pairs, chips), dma(pairs, chips),
-            dma(tiles, n_sp), dma(tiles, n_sp), dma(tiles, n_sp), dma(tiles, n_sp),
+            *[dma(tiles, pieces)] * 6,
             dma(pairs), dma(pairs), dma(pairs, chips), dma(pairs, chips),
         ],
         compiler_params=pltpu.CompilerParams(
-            collective_id=0, has_side_effects=True, vmem_limit_bytes=62 * 1024 * 1024
+            collective_id=0, has_side_effects=True, vmem_limit_bytes=50 * 1024 * 1024
         ),
         name="fused_backward",
-    )(
+    )(*(pltpu.with_memory_space_constraint(jnp.asarray(x), pltpu.HBM) for x in (
         latent, rope_t, kv_gain.reshape(1, -1), np.tile(cosine, (1, 4)),
         np.concatenate([-sine, sine, -sine, sine], axis=1),
         np.ascontiguousarray(cosine.T), np.ascontiguousarray(sine.T),
         queries, out_grad, key_up, value_up,
-    )
+    )))
 
 
 def write_kernel(dq_ref, grad_ref, low_ref, dq_out, lat_out, rot_out, key_out, value_out, rot, sem):

time: 76.8 us -> 61.4 us (0.80)
  Pallas kernels: 72 us -> 60.6 us
  local copies, waits for them, and re-layouts: 3.9 us -> 0 us
    pallas_call x1, Pallas kernels: 70.1 us -> 58.7 us  [fused(): pl.pallas_call(functools.partial(kernel, block, grad_scale, n_sp, n_dp),...]
    unnamed x6 -> x0, local copies, waits for them, and re-layouts: 3.9 us -> none
where the time goes in v2:
time: 61.4 us; the launch traced here: 61.2 us
  Pallas kernels  60.6 us (99%)
  between operations  0.64 us (1%)
    pallas_call x1, Pallas kernels, fused(): pl.pallas_call(functools.partial(kernel, block, grad_scale, n_sp, n_dp),...  58.7 us
    pallas_call x1, Pallas kernels, write(): pl.pallas_call(write_kernel, in_specs=[pl.BlockSpec(memory_space=pltpu.VM...  1.9 us

profile of v2, /device:TPU:0, one launch (start us, length us, event | category | flops | bytes accessed | tf_op | source)
XLA Modules:
  0.0 61.2 jit_solution(6123933165655149344)
XLA Ops:
  0.6 58.7 %fused_backward.1 = (bf16[768,1536]{1,0:T(8,128)(2,1)S(1)}, f32[2,64,1024]{2,1,0:T(8,128)S(1)}, bf16[3,4,64,640]{3,2,1,0:T(8,128)(2,1)S(1)}) custom-call(bf16[768,512]{1,0:T(8,128)(2,1)} %bitcast.16, bf16[64,768]{1,0:T(8,128)(2,1)} %bitcast.17, f32[1,512]{1,0:T(1,128)} %bitcast.18, f32[768,128]{1,0:T(8,128)} %constant.8.clone.cos_hbm, ...), custom_call_target="tpu_custom_call" | custom-call | tf_op jit(solution)/shard_map/fused_backward/pallas_call | solution.py:430
  59.3 1.9 %write_outputs.1 = (bf16[768,1536]{1,0:T(8,128)(2,1)}, bf16[768,512]{1,0:T(8,128)(2,1)}, bf16[64,768]{1,0:T(8,128)(2,1)}, f32[64,1024]{1,0:T(8,128)}, f32[64,1024]{1,0:T(8,128)}) custom-call(bf16[768,1536]{1,0:T(8,128)(2,1)S(1)} %get-tuple-element.13.dq_ref, f32[2,64,1024]{2,1,0:T(8,128)S(1)} %get-tuple-element.14.grad_ref, bf16[768,640]{1,0:T(8,128)(2,1)S(1)} %bitcast.13), custom_call_target="tpu_custom_call" | custom-call | tf_op jit(solution)/shard_map/write_outputs/pallas_call | solution.py:484

commit v3 on v2

--- a/solution.py
+++ b/solution.py
@@ -41,6 +41,16 @@
     return jnp.where(lane % ROPE_DIM < ROPE_DIM // 2, pltpu.roll(x, 96, 1), pltpu.roll(x, 32, 1))
 
 
+def flat(wide):
+    count = wide.shape[0] // 8
+    return jnp.concatenate([wide[8 * a:8 * a + 8] for a in range(count)], axis=1)
+
+
+def unflat(rows):
+    count = rows.shape[1] // 128
+    return jnp.concatenate([rows[:, 128 * a:128 * a + 128] for a in range(count)], axis=0)
+
+
 def each(first, count, act):
     def body(k, carry):
         act(k)
@@ -53,7 +63,7 @@
     latent_hbm, rope_hbm, gain_hbm, cos_hbm, sin_hbm, cos_t_hbm, sin_t_hbm,
     q_hbm, do_hbm, wk_hbm, wv_hbm,
     dq_ref, grad_ref, low_ref,
-    lat, rope, gain, cosw, sinw, cost, sint, qin, doin, w,
+    lat, rope, gain, cosw, sinw, cost, sint, doin, w, w_t,
     comp, comp_t, krot, krot_t, ku, kt, vals, qu, pt, dst, dkv, acc, rot_acc,
     part, got_in, got_mid, dwbuf, got_near, red, got_far,
     in_sem, w_sem, q_sem, do_sem,
@@ -63,7 +73,7 @@
     chips = n_dp // 2
     chip, core = dp // 2, lax.rem(dp, 2)
     partner = chip * 2 + 1 - core
-    pairs, length = qin.shape[0], qin.shape[1]
+    pairs, length = doin.shape[0], doin.shape[1]
     width = lat.shape[1]
     tiles = length // block
     pieces = part.shape[1]
@@ -106,8 +116,8 @@
             (cos_hbm, cosw), (sin_hbm, sinw)))]
 
     def q_load(p):
-        return pltpu.make_async_copy(
-            q_hbm.at[:, pl.ds(pl.multiple_of(p * 2 * QK, 128), 2 * QK)], qin.at[p], q_sem.at[p])
+        cols = pl.ds(pl.multiple_of(p * 2 * QK, 128), 2 * QK)
+        return pltpu.make_async_copy(q_hbm.at[:, cols], dq_ref.at[:, cols], q_sem.at[p])
 
     def do_load(p):
         return pltpu.make_async_copy(
@@ -161,13 +171,14 @@
 
     def turn_queries(p):
         q_load(p).wait()
-        mid = qin[p, :, 128:256].astype(jnp.float32)
-        last = qin[p, :, 256:384].astype(jnp.float32)
+        third = lambda n: dq_ref[:, pl.ds(pl.multiple_of(p * 2 * QK + n * 128, 128), 128)]
+        mid = third(1).astype(jnp.float32)
+        last = third(2).astype(jnp.float32)
         low = lax.broadcasted_iota(jnp.int32, mid.shape, 1) < 64
         plain = jnp.where(low, pltpu.roll(mid, 64, 1), pltpu.roll(last, 64, 1))
         both = jnp.where(low, mid, last)
         rot = both * cosw[...] + swap_halves(both) * sinw[...]
-        qu[2 * p, :, :NOPE_DIM] = qin[p, :, :128]
+        qu[2 * p, :, :NOPE_DIM] = third(0)
         qu[2 * p, :, NOPE_DIM:] = rot[:, :ROPE_DIM].astype(jnp.bfloat16)
         qu[2 * p + 1, :, :NOPE_DIM] = plain.astype(jnp.bfloat16)
         qu[2 * p + 1, :, NOPE_DIM:] = pltpu.roll(rot, 64, 1)[:, :ROPE_DIM].astype(jnp.bfloat16)
@@ -187,27 +198,26 @@
             kt[2 * p + h, :NOPE_DIM, :] = keys_t[h * NOPE_DIM:(h + 1) * NOPE_DIM, :]
             kt[2 * p + h, NOPE_DIM:, :] = krot_t[...]
 
-    def attend(i, p):
+    def attend(i, p, h):
         rows = slice(i * block, (i + 1) * block)
         n = (i + 1) * block
-        for h in range(2):
-            cols = slice(h * VALUE_DIM, (h + 1) * VALUE_DIM)
-            scores = dot_nt(ku[2 * p + h, :n, :], qu[2 * p + h, rows, :])
-            key_at = lax.broadcasted_iota(jnp.int32, (block, block), 0)
-            query_at = lax.broadcasted_iota(jnp.int32, (block, block), 1)
-            diag = jnp.where(key_at <= query_at, scores[n - block:], -jnp.inf)
-            scores = diag if i == 0 else jnp.concatenate([scores[:n - block], diag], axis=0)
-            top = jnp.max(scores, axis=0, keepdims=True)
-            e = jnp.exp2((scores - top) * (scale * LOG2E))
-            r = 1.0 / jnp.sum(e, axis=0, keepdims=True)
-            prob_grad = dot_nt(vals[p, :n, cols], doin[p, rows, cols])
-            center = jnp.sum(e * prob_grad, axis=0, keepdims=True) * r
-            prob = (e * r).astype(jnp.bfloat16)
-            grad = (e * (r * scale) * (prob_grad - center)).astype(jnp.bfloat16)
-            for j in range(i + 1):
-                at = slice((i - j) * block, (i - j + 1) * block)
-                pt[j][2 * p + h, :, at] = prob[j * block:(j + 1) * block]
-                dst[j][2 * p + h, :, at] = grad[j * block:(j + 1) * block]
+        cols = slice(h * VALUE_DIM, (h + 1) * VALUE_DIM)
+        scores = dot_nt(ku[2 * p + h, :n, :], qu[2 * p + h, rows, :])
+        key_at = lax.broadcasted_iota(jnp.int32, (block, block), 0)
+        query_at = lax.broadcasted_iota(jnp.int32, (block, block), 1)
+        diag = jnp.where(key_at <= query_at, scores[n - block:], -jnp.inf)
+        scores = diag if i == 0 else jnp.concatenate([scores[:n - block], diag], axis=0)
+        top = jnp.max(scores, axis=0, keepdims=True)
+        e = jnp.exp2((scores - top) * (scale * LOG2E))
+        r = 1.0 / jnp.sum(e, axis=0, keepdims=True)
+        prob_grad = dot_nt(vals[p, :n, cols], doin[p, rows, cols])
+        center = jnp.sum(e * prob_grad, axis=0, keepdims=True) * r
+        prob = (e * r).astype(jnp.bfloat16)
+        grad = (e * (r * scale) * (prob_grad - center)).astype(jnp.bfloat16)
+        for j in range(i + 1):
+            at = slice((i - j) * block, (i - j + 1) * block)
+            pt[j][2 * p + h, :, at] = prob[j * block:(j + 1) * block]
+            dst[j][2 * p + h, :, at] = grad[j * block:(j + 1) * block]
 
     def key_block(i, p):
         rows = slice(i * block, (i + 1) * block)
@@ -220,7 +230,7 @@
             dkv[p, rows, (2 + h) * 128:(3 + h) * 128] = dv.astype(jnp.bfloat16)
             rot = dk[:, NOPE_DIM:] if rot is None else rot + dk[:, NOPE_DIM:]
         rot_acc[...] += rot
-        acc[...] += dot_nt(dkv[p, rows, :], w[p].reshape(width, 512))
+        acc[...] += dot(dkv[p, rows, :], w_t[p])
 
     def in_copy(i, q):
         return pltpu.make_async_remote_copy(
@@ -245,9 +255,12 @@
         pl.when(jnp.logical_not(at_middle))(lambda: in_copy(i, q).start())
 
     def send_part(i):
-        rot = rot_acc[...].astype(jnp.bfloat16)
-        whole = jnp.concatenate([acc[...].astype(jnp.bfloat16), rot, rot], axis=1)
-        part[i] = whole.reshape(pieces, rows_of, width + 128)
+        for q in range(pieces):
+            mine = slice(q * rows_of, (q + 1) * rows_of)
+            part[i, q, :rows_of] = acc[mine].astype(jnp.bfloat16)
+            rot = rot_acc[mine]
+            wide = jnp.concatenate([rot[:rows_of // 2], rot[rows_of // 2:]], axis=1)
+            part[i, q, rows_of:] = flat(wide).astype(jnp.bfloat16)
         def go():
             for q in range(pieces):
                 go_in(i, q)
@@ -267,13 +280,13 @@
             mine = slice(i * block + q * rows_of, i * block + (q + 1) * rows_of)
             raw = lat[mine, :].astype(jnp.float32)
             inverse = lax.rsqrt(jnp.mean(raw * raw, axis=-1, keepdims=True) + norm_eps)
-            mixed = total[:, :width] * gain[...]
+            mixed = total[:rows_of] * gain[...]
             spread = jnp.mean(raw * mixed, axis=-1, keepdims=True)
-            low_ref[i, q, :, :width] = (inverse * mixed - raw * inverse**3 * spread).astype(jnp.bfloat16)
-            rot = total[:, width:]
-            low_ref[i, q, :, width:] = (
-                rot * cosw[mine, :] - swap_halves(rot) * sinw[mine, :]
-            ).astype(jnp.bfloat16)
+            low_ref[i, q, :rows_of] = (inverse * mixed - raw * inverse**3 * spread).astype(jnp.bfloat16)
+            rot = unflat(total[rows_of:])
+            left = lax.broadcasted_iota(jnp.int32, rot.shape, 1) < ROPE_DIM
+            c, s = (jnp.where(left, t[:rows_of // 2], t[rows_of // 2:]) for t in (cosw[mine, :], sinw[mine, :]))
+            low_ref[i, q, rows_of:] = flat(rot * c - swap_halves(rot) * s).astype(jnp.bfloat16)
             pl.when(jnp.logical_not(at_end))(lambda: out_copy(i, q).start())
         pl.when(at_middle)(go)
 
@@ -339,12 +352,12 @@
     for i in range(tiles - 1, 0, -1):
         if i > 1:
             stage(merge, i, (i - 1, 2), (i - 1, 3), ("sent", i - 1), (i - 2, 0))
-            stage(finish, i, (i - 2, 0), (i - 2, 1), (i - 2, 2), (i - 2, 3))
+            stage(finish, i, (i - 2, 1), (i - 2, 2), (i - 2, 3), ("w", 0))
         else:
-            stage(merge, 1, (0, 2), (0, 3), ("w", 1), ("w", 3))
-            stage(finish, 1, ("w", 3), "grads", ("q2", 2), ("q1", 1))
-    stage(merge, 0, ("q2", 2), ("q1", 2), "end", "end3")
-    stage(finish, 0, "end1", "end4", "end5", "end6")
+            stage(merge, 1, (0, 2), (0, 3), ("w", 0), ("w", 2))
+            stage(finish, 1, ("w", 3), "grads", ("q2", 1), ("q2", 3))
+    stage(merge, 0, ("q2", 1), ("q2", 3), ("q1", 1), ("q1", 3))
+    stage(finish, 0, ("q0", 0), ("q0", 3), "end", "end")
 
     def run(key):
         for act in stages.pop(key, []):
@@ -363,9 +376,11 @@
         def step(p, i=i):
             if i == tiles - 1:
                 project(p)
-            attend(i, p)
+            attend(i, p, 0)
             if i == tiles - 1:
                 pl.when(p + 1 < pairs)(lambda: forward(p + 1))
+                w_t[p] = w[p].reshape(width, 512).T
+            attend(i, p, 1)
             key_block(i, p)
             run_in(i, p)
         each(0, pairs, step)
@@ -374,10 +389,11 @@
 
     def grads(p):
         weight_grad(p)
-        pl.when(p > 0)(lambda: chip_grad(p - 1))
+        pl.when(p > 1)(lambda: chip_grad(p - 2))
         run_in("w", p)
     each(0, pairs, grads)
-    chip_grad(pairs - 1)
+    for p in range(max(pairs - 2, 0), pairs):
+        chip_grad(p)
     run("grads")
 
     for i in reversed(range(tiles)):
@@ -418,7 +434,8 @@
     block = 256
     tiles = length // block
     pieces = 4
-    piece = (tiles, pieces, block // pieces, width + 128)
+    rows = block // pieces
+    piece = (tiles, pieces, rows + rows * ROPE_DIM // width, width)
     depth = key_up.shape[0]
     cosine, sine = rope_tables(length)
     bf, f32 = jnp.bfloat16, jnp.float32
@@ -439,7 +456,7 @@
         scratch_shapes=[
             V((length, width), bf), V((ROPE_DIM, length), bf), V((1, width), f32),
             V((length, 128), f32), V((length, 128), f32), V((32, length), f32), V((32, length), f32),
-            V((pairs, length, 2 * QK), bf), V((pairs, length, 256), bf), V((pairs, n_dp, depth, 512), bf),
+            V((pairs, length, 256), bf), V((pairs, n_dp, depth, 512), bf), V((pairs, 512, width), bf),
             V((length, width), bf), V((width, length), bf), V((length, 128), bf), V((ROPE_DIM, length), bf),
             V((heads, length, QK), bf), V((heads, QK, length), bf), V((pairs, length, 256), bf),
             V((heads, length, QK), bf), triangle, triangle,
@@ -465,21 +482,29 @@
 
 
 def write_kernel(dq_ref, grad_ref, low_ref, dq_out, lat_out, rot_out, key_out, value_out, rot, sem):
-    width = lat_out.shape[1]
+    count, rows = low_ref.shape[0], lat_out.shape[0] // low_ref.shape[0]
     copies = [
         pltpu.make_async_copy(src, dst_, sem.at[j]) for j, (src, dst_) in enumerate((
-            (dq_ref, dq_out), (low_ref.at[:, pl.ds(0, width)], lat_out),
-            (grad_ref.at[0], key_out), (grad_ref.at[1], value_out), (rot, rot_out)))]
-    for copy in copies[:4]:
-        copy.start()
-    rot[...] = low_ref[:, width:].astype(jnp.float32).T[:ROPE_DIM].astype(jnp.bfloat16)
-    copies[4].start()
+            (dq_ref, dq_out), (grad_ref.at[0], key_out), (grad_ref.at[1], value_out), (rot, rot_out)))]
+    copies += [
+        pltpu.make_async_copy(
+            low_ref.at[j, pl.ds(0, rows)], lat_out.at[pl.ds(j * rows, rows)], sem.at[4 + j])
+        for j in range(count)]
+    for j, copy in enumerate(copies):
+        if j != 3:
+            copy.start()
+    turned = []
+    for j in range(count):
+        wide = unflat(low_ref[j, rows:].astype(jnp.float32))
+        turned += [wide, pltpu.roll(wide, 64, 1)]
+    rot[...] = jnp.concatenate(turned, axis=0).T[:ROPE_DIM].astype(jnp.bfloat16)
+    copies[3].start()
     for copy in copies:
         copy.wait()
 
 
-def write(dq, grad, low):
-    length, width = low.shape[0], low.shape[1] - 128
+def write(dq, grad, low, length):
+    width = low.shape[2]
     bf, f32 = jnp.bfloat16, jnp.float32
     return pl.pallas_call(
         write_kernel,
@@ -492,7 +517,7 @@
             jax.ShapeDtypeStruct(grad.shape[1:], f32),
             jax.ShapeDtypeStruct(grad.shape[1:], f32),
         ],
-        scratch_shapes=[pltpu.VMEM((ROPE_DIM, length), bf), pltpu.SemaphoreType.DMA((5,))],
+        scratch_shapes=[pltpu.VMEM((ROPE_DIM, length), bf), pltpu.SemaphoreType.DMA((4 + low.shape[0],))],
         compiler_params=pltpu.CompilerParams(vmem_limit_bytes=16 * 1024 * 1024),
         name="write_outputs",
     )(dq, grad, low)
@@ -506,7 +531,7 @@
     dq, grad, low = fused(
         queries[0], out_grad[0], latent[0], rope_t, kv_gain, key_up, value_up, grad_scale, n_sp, n_dp
     )
-    dq, lat, rot_t, key_grad, value_grad = write(dq, grad, low.reshape(length, width + 128))
+    dq, lat, rot_t, key_grad, value_grad = write(dq, grad, low.reshape(-1, *low.shape[2:]), length)
     return dq[None], lat[None], jnp.swapaxes(rot_t[None], 1, 2), key_grad, value_grad
 
 

time: 61.4 us -> 58.3 us (0.950)
  Pallas kernels: 60.6 us -> 57.5 us
    pallas_call x1, Pallas kernels: 58.7 us -> 55.5 us  [fused(): pl.pallas_call(functools.partial(kernel, block, grad_scale, n_sp, n_dp),...]
where the time goes in v3:
time: 58.3 us; the launch traced here: 58.1 us
  Pallas kernels  57.5 us (99%)
  between operations  0.64 us (1%)
    pallas_call x1, Pallas kernels, fused(): pl.pallas_call(functools.partial(kernel, block, grad_scale, n_sp, n_dp),...  55.5 us
    pallas_call x1, Pallas kernels, write(): pl.pallas_call(write_kernel, in_specs=[pl.BlockSpec(memory_space=pltpu.VM...  2.01 us

profile of v3, /device:TPU:0, one launch (start us, length us, event | category | flops | bytes accessed | tf_op | source)
XLA Modules:
  0.0 58.1 jit_solution(12500164628437749957)
XLA Ops:
  0.6 55.5 %fused_backward.1 = (bf16[768,1536]{1,0:T(8,128)(2,1)S(1)}, f32[2,64,1024]{2,1,0:T(8,128)S(1)}, bf16[3,4,72,512]{3,2,1,0:T(8,128)(2,1)S(1)}) custom-call(bf16[768,512]{1,0:T(8,128)(2,1)} %bitcast.16, bf16[64,768]{1,0:T(8,128)(2,1)} %bitcast.17, f32[1,512]{1,0:T(1,128)} %bitcast.18, f32[768,128]{1,0:T(8,128)} %constant.8.clone.cos_hbm, ...), custom_call_target="tpu_custom_call" | custom-call | tf_op jit(solution)/shard_map/fused_backward/pallas_call | solution.py:447
  56.1 2.0 %write_outputs.1 = (bf16[768,1536]{1,0:T(8,128)(2,1)}, bf16[768,512]{1,0:T(8,128)(2,1)}, bf16[64,768]{1,0:T(8,128)(2,1)}, f32[64,1024]{1,0:T(8,128)}, f32[64,1024]{1,0:T(8,128)}) custom-call(bf16[768,1536]{1,0:T(8,128)(2,1)S(1)} %get-tuple-element.13.dq_ref, f32[2,64,1024]{2,1,0:T(8,128)S(1)} %get-tuple-element.14.grad_ref, bf16[12,72,512]{2,1,0:T(8,128)(2,1)S(1)} %bitcast.13), custom_call_target="tpu_custom_call" | custom-call | tf_op jit(solution)/shard_map/write_outputs/pallas_call | solution.py:509

commit v4 on v3

--- a/solution.py
+++ b/solution.py
@@ -63,11 +63,11 @@
     latent_hbm, rope_hbm, gain_hbm, cos_hbm, sin_hbm, cos_t_hbm, sin_t_hbm,
     q_hbm, do_hbm, wk_hbm, wv_hbm,
     dq_ref, grad_ref, low_ref,
-    lat, rope, gain, cosw, sinw, cost, sint, doin, w, w_t,
+    lat, rope, gain, cosw, sinw, cost, sint, doin, w,
     comp, comp_t, krot, krot_t, ku, kt, vals, qu, pt, dst, dkv, acc, rot_acc,
     part, got_in, got_mid, dwbuf, got_near, red, got_far,
-    in_sem, w_sem, q_sem, do_sem,
-    far_s, far_r, near_s, near_r, a_s, a_r, m_s, m_r, b_s, b_r, c_s, c_r, d_s, d_r,
+    in_sem, w_sem, do_sem,
+    far_s, far_r, near_s, near_r, a_s, a_r, b_s, b_r, c_s, c_r, d_s, d_r,
 ):
     sp, dp = lax.axis_index("sp"), lax.axis_index("dp")
     chips = n_dp // 2
@@ -94,7 +94,7 @@
         hbm = (wk_hbm, wv_hbm)[t]
         return pltpu.make_async_copy(
             hbm.at[:, pl.ds(pl.multiple_of(p * 256, 256), 256)],
-            w.at[p, dp, :, pl.ds(t * 256, 256)], w_sem.at[p, t])
+            w.at[p, dp, :, pl.ds(t * 256, 256)], w_sem.at[0])
 
     for t in range(2):
         each(0, pairs, lambda p: w_load(p, t).start())
@@ -112,37 +112,31 @@
 
     loads = [
         pltpu.make_async_copy(src, dst_, in_sem.at[j]) for j, (src, dst_) in enumerate((
-            (latent_hbm, lat), (gain_hbm, gain), (rope_hbm, rope), (cos_t_hbm, cost), (sin_t_hbm, sint),
+            (q_hbm, dq_ref), (latent_hbm, lat), (gain_hbm, gain), (rope_hbm, rope), (cos_t_hbm, cost), (sin_t_hbm, sint),
             (cos_hbm, cosw), (sin_hbm, sinw)))]
-
-    def q_load(p):
-        cols = pl.ds(pl.multiple_of(p * 2 * QK, 128), 2 * QK)
-        return pltpu.make_async_copy(q_hbm.at[:, cols], dq_ref.at[:, cols], q_sem.at[p])
 
     def do_load(p):
         return pltpu.make_async_copy(
-            do_hbm.at[:, pl.ds(pl.multiple_of(p * 256, 256), 256)], doin.at[p], do_sem.at[p])
+            do_hbm.at[:, pl.ds(pl.multiple_of(p * 256, 256), 256)], doin.at[p], do_sem.at[0])
 
     for copy in loads:
         copy.start()
-    each(0, pairs, lambda p: q_load(p).start())
     each(0, pairs, lambda p: do_load(p).start())
 
     def far(p, k):
         return pltpu.make_async_remote_copy(
             src_ref=w.at[p, dp], dst_ref=w.at[p, dp],
-            send_sem=far_s.at[p, k], recv_sem=far_r.at[p, k],
+            send_sem=far_s.at[0], recv_sem=far_r.at[p],
             device_id={"dp": other(k)}, device_id_type=MESH)
 
     def near(p, k):
         row = source(k)
         return pltpu.make_async_remote_copy(
             src_ref=w.at[p, row], dst_ref=w.at[p, row],
-            send_sem=near_s.at[p, k], recv_sem=near_r.at[p, k],
+            send_sem=near_s.at[0], recv_sem=near_r.at[p],
             device_id={"dp": partner}, device_id_type=MESH)
 
-    for t in range(2):
-        each(0, pairs, lambda p: w_load(p, t).wait())
+    pltpu.make_async_copy(w.at[:, dp], w.at[:, dp], w_sem.at[0]).wait()
     pl.semaphore_wait(barrier, chips + jnp.where(at_end, 1, 2))
 
     def send_weights(p):
@@ -150,11 +144,12 @@
         near(p, 0).start()
     each(0, pairs, send_weights)
 
+    def blocks_in(ref, sem):
+        return pltpu.make_async_copy(ref, ref, sem)
+
     def forward(p):
-        def go(k):
-            far(p, k).wait_recv()
-            near(p, k).start()
-        each(1, chips, go)
+        blocks_in(w.at[p, pl.ds(0, chips - 1)], far_r.at[p]).wait()
+        each(1, chips, lambda k: near(p, k).start())
 
     for copy in loads:
         copy.wait()
@@ -170,7 +165,6 @@
     krot[...] = jnp.concatenate([turned, turned], axis=0).T.astype(jnp.bfloat16)
 
     def turn_queries(p):
-        q_load(p).wait()
         third = lambda n: dq_ref[:, pl.ds(pl.multiple_of(p * 2 * QK + n * 128, 128), 128)]
         mid = third(1).astype(jnp.float32)
         last = third(2).astype(jnp.float32)
@@ -183,20 +177,17 @@
         qu[2 * p + 1, :, :NOPE_DIM] = plain.astype(jnp.bfloat16)
         qu[2 * p + 1, :, NOPE_DIM:] = pltpu.roll(rot, 64, 1)[:, :ROPE_DIM].astype(jnp.bfloat16)
     each(0, pairs, turn_queries)
-    each(0, pairs, lambda p: do_load(p).wait())
+    pltpu.make_async_copy(doin, doin, do_sem.at[0]).wait()
 
     def project(p):
-        each(0, chips, lambda k: near(p, k).wait_recv())
+        blocks_in(w.at[p, pl.ds(0, chips)], near_r.at[p]).wait()
         both = dot(comp[...], w[p].reshape(width, 512))
         keys = both[:, :256]
-        keys_t = keys.T.astype(jnp.bfloat16)
         keys = keys.astype(jnp.bfloat16)
         vals[p] = both[:, 256:].astype(jnp.bfloat16)
         for h in range(2):
             ku[2 * p + h, :, :NOPE_DIM] = keys[:, h * NOPE_DIM:(h + 1) * NOPE_DIM]
             ku[2 * p + h, :, NOPE_DIM:] = krot[:, :ROPE_DIM]
-            kt[2 * p + h, :NOPE_DIM, :] = keys_t[h * NOPE_DIM:(h + 1) * NOPE_DIM, :]
-            kt[2 * p + h, NOPE_DIM:, :] = krot_t[...]
 
     def attend(i, p, h):
         rows = slice(i * block, (i + 1) * block)
@@ -230,24 +221,23 @@
             dkv[p, rows, (2 + h) * 128:(3 + h) * 128] = dv.astype(jnp.bfloat16)
             rot = dk[:, NOPE_DIM:] if rot is None else rot + dk[:, NOPE_DIM:]
         rot_acc[...] += rot
-        acc[...] += dot(dkv[p, rows, :], w_t[p])
 
     def in_copy(i, q):
         return pltpu.make_async_remote_copy(
             src_ref=part.at[i, q], dst_ref=got_in.at[i, q],
-            send_sem=a_s.at[i, q], recv_sem=a_r.at[i, q],
+            send_sem=a_s.at[0], recv_sem=a_r.at[i, q],
             device_id={"sp": inward}, device_id_type=MESH)
 
     def mid_copy(i, q):
         return pltpu.make_async_remote_copy(
             src_ref=part.at[i, q], dst_ref=got_mid.at[i, q],
-            send_sem=m_s.at[i, q], recv_sem=m_r.at[i, q],
+            send_sem=a_s.at[0], recv_sem=b_r.at[i, q],
             device_id={"sp": inward}, device_id_type=MESH)
 
     def out_copy(i, q):
         return pltpu.make_async_remote_copy(
             src_ref=low_ref.at[i, q], dst_ref=low_ref.at[i, q],
-            send_sem=b_s.at[i, q], recv_sem=b_r.at[i, q],
+            send_sem=b_s.at[0], recv_sem=b_r.at[i, q],
             device_id={"sp": outward}, device_id_type=MESH)
 
     def go_in(i, q):
@@ -255,6 +245,11 @@
         pl.when(jnp.logical_not(at_middle))(lambda: in_copy(i, q).start())
 
     def send_part(i):
+        total = None
+        for p in range(pairs):
+            term = dot_nt(dkv[p, i * block:(i + 1) * block, :], w[p].reshape(width, 512))
+            total = term if total is None else total + term
+        acc[...] = total
         for q in range(pieces):
             mine = slice(q * rows_of, (q + 1) * rows_of)
             part[i, q, :rows_of] = acc[mine].astype(jnp.bfloat16)
@@ -296,21 +291,16 @@
             pl.when(jnp.logical_not(at_end))(lambda: out_copy(i, q).start())
         pl.when(jnp.logical_not(at_middle))(go)
 
-    def drain_rows(i, q):
-        pl.when(at_middle)(lambda: mid_copy(i, q).wait_send())
-        pl.when(jnp.logical_not(at_middle))(lambda: in_copy(i, q).wait_send())
-        pl.when(jnp.logical_not(at_end))(lambda: out_copy(i, q).wait_send())
-
     def near_grad(p):
         return pltpu.make_async_remote_copy(
             src_ref=dwbuf.at[p, 1 - core], dst_ref=got_near.at[p],
-            send_sem=c_s.at[p], recv_sem=c_r.at[p],
+            send_sem=c_s.at[0], recv_sem=c_r.at[p],
             device_id={"dp": partner}, device_id_type=MESH)
 
     def far_grad(p, k):
         return pltpu.make_async_remote_copy(
             src_ref=red.at[p, chip_at(k)], dst_ref=got_far.at[p, k],
-            send_sem=d_s.at[p, k], recv_sem=d_r.at[p, k],
+            send_sem=d_s.at[0], recv_sem=d_r.at[p],
             device_id={"dp": other(k)}, device_id_type=MESH)
 
     def weight_grad(p):
@@ -331,6 +321,10 @@
         n = (i + 1) * block
         parts = []
         for h in range(2):
+            if i == tiles - 1:
+                plain = ku[2 * p + h, :, :NOPE_DIM].astype(jnp.float32)
+                kt[2 * p + h, :NOPE_DIM, :] = plain.T.astype(jnp.bfloat16)
+                kt[2 * p + h, NOPE_DIM:, :] = krot_t[...]
             g = dot(kt[2 * p + h, :, :n], jnp.concatenate(
                 [dst[j][2 * p + h, :, (i - j) * block:(i - j + 1) * block] for j in range(i + 1)], axis=0))
             a = g[NOPE_DIM:NOPE_DIM + 32]
@@ -349,15 +343,15 @@
             key = phase if at is None else (phase, min(at, last))
             stages.setdefault(key, []).append(functools.partial(act, i, q))
 
+    stage(merge, 0, ("w", 1), ("w", 3), ("q2", 0), ("q2", 3))
     for i in range(tiles - 1, 0, -1):
         if i > 1:
             stage(merge, i, (i - 1, 2), (i - 1, 3), ("sent", i - 1), (i - 2, 0))
-            stage(finish, i, (i - 2, 1), (i - 2, 2), (i - 2, 3), ("w", 0))
+            stage(finish, i, (i - 2, 0), (i - 2, 1), (i - 2, 2), (i - 2, 3))
         else:
-            stage(merge, 1, (0, 2), (0, 3), ("w", 0), ("w", 2))
-            stage(finish, 1, ("w", 3), "grads", ("q2", 1), ("q2", 3))
-    stage(merge, 0, ("q2", 1), ("q2", 3), ("q1", 1), ("q1", 3))
-    stage(finish, 0, ("q0", 0), ("q0", 3), "end", "end")
+            stage(merge, 1, (0, 1), (0, 2), (0, 3), ("w", 0))
+            stage(finish, 1, ("w", 1), ("w", 2), ("w", 3), "grads")
+    stage(finish, 0, ("q2", 1), ("q1", 0), ("q0", 0), "end")
 
     def run(key):
         for act in stages.pop(key, []):
@@ -370,30 +364,35 @@
 
     forward(0)
     for i in reversed(range(tiles)):
-        acc[...] = jnp.zeros_like(acc)
         rot_acc[...] = jnp.zeros_like(rot_acc)
 
         def step(p, i=i):
             if i == tiles - 1:
                 project(p)
+                pl.when(jnp.logical_and(p > 0, p < last))(lambda: forward(p + 1))
             attend(i, p, 0)
-            if i == tiles - 1:
-                pl.when(p + 1 < pairs)(lambda: forward(p + 1))
-                w_t[p] = w[p].reshape(width, 512).T
             attend(i, p, 1)
+            if i == tiles - 1 and last > 0:
+                pl.when(p == 0)(lambda: forward(1))
             key_block(i, p)
             run_in(i, p)
+            if i == 0:
+                pl.when(p == last)(lambda: weight_grad(0))
         each(0, pairs, step)
         send_part(i)
         run(("sent", min(i, last)))
 
+    run(("w", 0))
+
     def grads(p):
         weight_grad(p)
-        pl.when(p > 1)(lambda: chip_grad(p - 2))
+        pl.when(p == 1)(lambda: chip_grad(0))
+        pl.when(p > 2)(lambda: chip_grad(p - 2))
         run_in("w", p)
-    each(0, pairs, grads)
-    for p in range(max(pairs - 2, 0), pairs):
-        chip_grad(p)
+    each(1, pairs, grads)
+    for p in range(pairs):
+        if p >= pairs - 2 and not (p == 0 and pairs > 1):
+            chip_grad(p)
     run("grads")
 
     for i in reversed(range(tiles)):
@@ -406,24 +405,23 @@
     assert not stages
 
     def add(p):
+        blocks_in(got_far.at[p, pl.ds(1, chips - 1)], d_r.at[p]).wait()
         total = red[p, chip].astype(jnp.float32)
         for k in range(1, chips):
-            far_grad(p, k).wait()
             total = total + got_far[p, k].astype(jnp.float32)
         cols = pl.ds(pl.multiple_of(p * 256, 256), 256)
         grad_ref[0, :, cols] = total[:, :256]
         grad_ref[1, :, cols] = total[:, 256:]
-        near_grad(p).wait_send()
-        def drain(k):
-            far(p, k).wait_send()
-            near(p, k).wait_send()
-        each(1, chips, drain)
-        near(p, 0).wait_send()
     each(0, pairs, add)
+    blocks_in(w.at[:, pl.ds(0, chips - 1)], far_s.at[0]).wait()
+    blocks_in(w.at[:, pl.ds(0, chips)], near_s.at[0]).wait()
+    blocks_in(got_near, c_s.at[0]).wait()
+    blocks_in(red.at[:, pl.ds(0, chips - 1)], d_s.at[0]).wait()
+    blocks_in(part, a_s.at[0]).wait()
     for i in reversed(range(tiles)):
         for q in range(pieces):
             deliver(i, q)
-            drain_rows(i, q)
+    pl.when(jnp.logical_not(at_end))(lambda: blocks_in(part, b_s.at[0]).wait())
 
 
 def fused(queries, out_grad, latent, rope_t, kv_gain, key_up, value_up, grad_scale, n_sp, n_dp):
@@ -456,7 +454,7 @@
         scratch_shapes=[
             V((length, width), bf), V((ROPE_DIM, length), bf), V((1, width), f32),
             V((length, 128), f32), V((length, 128), f32), V((32, length), f32), V((32, length), f32),
-            V((pairs, length, 256), bf), V((pairs, n_dp, depth, 512), bf), V((pairs, 512, width), bf),
+            V((pairs, length, 256), bf), V((pairs, n_dp, depth, 512), bf),
             V((length, width), bf), V((width, length), bf), V((length, 128), bf), V((ROPE_DIM, length), bf),
             V((heads, length, QK), bf), V((heads, QK, length), bf), V((pairs, length, 256), bf),
             V((heads, length, QK), bf), triangle, triangle,
@@ -464,10 +462,10 @@
             V(piece, bf), V(piece, bf), V(piece, bf),
             V((pairs, 2, chips, depth, 512), bf), V((pairs, chips, depth, 512), bf),
             V((pairs, chips, depth, 512), bf), V((pairs, chips, depth, 512), bf),
-            dma(7), dma(pairs, 2), dma(pairs), dma(pairs),
-            dma(pairs, chips), dma(pairs, chips), dma(pairs, chips), dma(pairs, chips),
-            *[dma(tiles, pieces)] * 6,
-            dma(pairs), dma(pairs), dma(pairs, chips), dma(pairs, chips),
+            dma(8), dma(1), dma(1),
+            dma(1), dma(pairs), dma(1), dma(pairs),
+            dma(1), dma(tiles, pieces), dma(1), dma(tiles, pieces),
+            dma(1), dma(pairs), dma(1), dma(pairs),
         ],
         compiler_params=pltpu.CompilerParams(
             collective_id=0, has_side_effects=True, vmem_limit_bytes=50 * 1024 * 1024

time: 58.3 us -> 56.6 us (0.971)
  Pallas kernels: 57.5 us -> 55.8 us
    pallas_call x1, Pallas kernels: 55.5 us -> 53.8 us  [fused(): pl.pallas_call(functools.partial(kernel, block, grad_scale, n_sp, n_dp),...]
where the time goes in v4:
time: 56.6 us; the launch traced here: 56.4 us
  Pallas kernels  55.8 us (99%)
  between operations  0.64 us (1%)
    pallas_call x1, Pallas kernels, fused(): pl.pallas_call(functools.partial(kernel, block, grad_scale, n_sp, n_dp),...  53.8 us
    pallas_call x1, Pallas kernels, write(): pl.pallas_call(write_kernel, in_specs=[pl.BlockSpec(memory_space=pltpu.VM...  2.01 us

profile of v4, /device:TPU:0, one launch (start us, length us, event | category | flops | bytes accessed | tf_op | source)
XLA Modules:
  0.0 56.4 jit_solution(422039191498608228)
XLA Ops:
  0.6 53.8 %fused_backward.1 = (bf16[768,1536]{1,0:T(8,128)(2,1)S(1)}, f32[2,64,1024]{2,1,0:T(8,128)S(1)}, bf16[3,4,72,512]{3,2,1,0:T(8,128)(2,1)S(1)}) custom-call(bf16[768,512]{1,0:T(8,128)(2,1)} %bitcast.16, bf16[64,768]{1,0:T(8,128)(2,1)} %bitcast.17, f32[1,512]{1,0:T(1,128)} %bitcast.18, f32[768,128]{1,0:T(8,128)} %constant.8.clone.cos_hbm, ...), custom_call_target="tpu_custom_call" | custom-call | tf_op jit(solution)/shard_map/fused_backward/pallas_call | solution.py:445
  54.4 2.0 %write_outputs.1 = (bf16[768,1536]{1,0:T(8,128)(2,1)}, bf16[768,512]{1,0:T(8,128)(2,1)}, bf16[64,768]{1,0:T(8,128)(2,1)}, f32[64,1024]{1,0:T(8,128)}, f32[64,1024]{1,0:T(8,128)}) custom-call(bf16[768,1536]{1,0:T(8,128)(2,1)S(1)} %get-tuple-element.13.dq_ref, f32[2,64,1024]{2,1,0:T(8,128)S(1)} %get-tuple-element.14.grad_ref, bf16[12,72,512]{2,1,0:T(8,128)(2,1)S(1)} %bitcast.13), custom_call_target="tpu_custom_call" | custom-call | tf_op jit(solution)/shard_map/write_outputs/pallas_call | solution.py:507
